TPU v7x, 32 devices: a whole 2x2x4 slice. The times are simulated.
32 devices in a mesh: tp: 8 (over z, y), dp: 4 (over x, core).
Axes of the slice: x: 2, y: 2, z: 4, core: 2. Of those that a mesh axis runs over, the one named last changes fastest.
Arguments:
- tokens: bfloat16 [192, 8448], P('dp', 'tp'), may hold values from -6 to 6
- gains: float32 [2, 8448], replicated, may hold values from 0.1 to 1.9
- w_input: bfloat16 [2, 8448, 12288], P(None, 'dp', 'tp'), may hold values from -0.0625 to 0.0625
- w_gating: bfloat16 [2, 8448, 12288], P(None, 'dp', 'tp'), may hold values from -0.0625 to 0.0625
- w_output: bfloat16 [2, 12288, 8448], P(None, 'tp'), may hold values from -0.21875 to 0.21875
- decay_rate: float32 [2, 768, 64], P(None, 'tp'), may hold values from 0.05 to 2
- frequency: float32 [2, 768, 64], P(None, 'tp'), may hold values from -3 to 3
- log_step: float32 [2, 768], P(None, 'tp'), may hold values from -2.3 to 0
- in_real: float32 [2, 768, 64, 16], P(None, 'tp'), may hold values from -1 to 1
- in_imag: float32 [2, 768, 64, 16], P(None, 'tp'), may hold values from -1 to 1
- readout_real_matrix: float32 [2, 768, 16, 64], P(None, 'tp'), may hold values from -0.5 to 0.5
- readout_imag_matrix: float32 [2, 768, 16, 64], P(None, 'tp'), may hold values from -0.5 to 0.5
- skip_gain: float32 [2, 12288], P(None, 'tp'), may hold values from -4 to 4
- state_real: float32 [2, 192, 768, 64], P(None, 'dp', 'tp'), may hold values from -6 to 6
- state_imag: float32 [2, 192, 768, 64], P(None, 'dp', 'tp'), may hold values from -6 to 6
Outputs:
- mixed: bfloat16 [192, 8448], P('dp', 'tp')
- next_real: float32 [2, 192, 768, 64], P(None, 'dp', 'tp')
- next_imag: float32 [2, 192, 768, 64], P(None, 'dp', 'tp')
All inputs are finite; a program needn't handle non-finite values.
Results may differ from a plain program's by a relative error of at most 0.008.
Values may be sent and summed in bfloat16 or wider, within the bound.
A program may use at most 256 MiB of HBM per device.

v0:
```python
import functools

import jax
import jax.numpy as jnp
from jax import lax
from jax.experimental import pallas as pl
from jax.experimental.pallas import tpu as pltpu
from jax.sharding import PartitionSpec as P

GS = 16
LAYERS = 2
MESH = pl.DeviceIdType.MESH
ANY = pl.BlockSpec(memory_space=pl.ANY)


def exchange_kernel(axis, n, count, *refs):
    ins, outs = refs[:count], refs[count : 2 * count]
    send, recv, local = refs[2 * count :]
    me = lax.axis_index(axis)
    barrier = pltpu.get_barrier_semaphore()
    for i in range(1, n):
        pl.semaphore_signal(
            barrier, inc=1, device_id={axis: lax.rem(me + i, n)}, device_id_type=MESH
        )
    own = [
        pltpu.make_async_copy(ins[k].at[me], outs[k].at[me], local.at[k]) for k in range(count)
    ]
    for copy in own:
        copy.start()
    pl.semaphore_wait(barrier, n - 1)
    copies = []
    for i in range(1, n):
        peer = lax.rem(me + i, n)
        for k in range(count):
            copy = pltpu.make_async_remote_copy(
                src_ref=ins[k].at[peer],
                dst_ref=outs[k].at[me],
                send_sem=send.at[k, i],
                recv_sem=recv.at[k, i],
                device_id={axis: peer},
                device_id_type=MESH,
            )
            copy.start()
            copies.append((i, k, copy))
    for copy in own:
        copy.wait()
    for i, k, copy in copies:
        copy.wait_send()
        source = lax.rem(me + n - i, n)
        pltpu.make_async_remote_copy(
            src_ref=ins[k].at[source],
            dst_ref=outs[k].at[source],
            send_sem=send.at[k, i],
            recv_sem=recv.at[k, i],
            device_id={axis: source},
            device_id_type=MESH,
        ).wait_recv()


def exchange(arrays, axis, n, ident):
    count = len(arrays)
    return pl.pallas_call(
        functools.partial(exchange_kernel, axis, n, count),
        out_shape=[jax.ShapeDtypeStruct(a.shape, a.dtype) for a in arrays],
        in_specs=[ANY] * count,
        out_specs=[ANY] * count,
        scratch_shapes=[
            pltpu.SemaphoreType.DMA((count, n)),
            pltpu.SemaphoreType.DMA((count, n)),
            pltpu.SemaphoreType.DMA((count,)),
        ],
        compiler_params=pltpu.CompilerParams(collective_id=ident, has_side_effects=True),
        name=f"exchange_{axis}_{ident}",
    )(*arrays)


def gather_kernel(tp, dp, x_ref, out_ref, send, recv):
    q = tp // dp
    t = lax.axis_index("tp")
    d = lax.axis_index("dp")
    group = t // q
    slot = lax.rem(t, q) * dp + d
    barrier = pltpu.get_barrier_semaphore()
    for h in range(q):
        for r in range(dp):
            source = d * q + h
            pl.semaphore_signal(
                barrier, inc=1, device_id={"tp": source, "dp": r}, device_id_type=MESH
            )

    pl.semaphore_wait(barrier, tp)

    def remote(i, index):
        return pltpu.make_async_remote_copy(
            src_ref=x_ref,
            dst_ref=out_ref.at[index],
            send_sem=send.at[i],
            recv_sem=recv.at[index],
            device_id={"tp": lax.rem(t + i, tp), "dp": group},
            device_id_type=MESH,
        )

    home = group == d

    @pl.when(home)
    def _():
        pltpu.make_async_copy(x_ref, out_ref.at[slot], recv.at[slot]).start()

    @pl.when(jnp.logical_not(home))
    def _():
        remote(0, slot).start()

    for i in range(1, tp):
        remote(i, slot).start()
    for i in range(1, tp):
        remote(i, slot).wait_send()

    @pl.when(jnp.logical_not(home))
    def _():
        remote(0, slot).wait_send()

    for index in range(tp):
        pltpu.make_async_copy(x_ref, out_ref.at[index], recv.at[index]).wait()


def gather(x, tp, dp, ident):
    return pl.pallas_call(
        functools.partial(gather_kernel, tp, dp),
        out_shape=jax.ShapeDtypeStruct((tp,) + x.shape, x.dtype),
        in_specs=[ANY],
        out_specs=ANY,
        scratch_shapes=[pltpu.SemaphoreType.DMA((tp,)), pltpu.SemaphoreType.DMA((tp,))],
        compiler_params=pltpu.CompilerParams(collective_id=ident, has_side_effects=True),
        name=f"gather_{ident}",
    )(x)


def state_kernel(many, u_ref, are_ref, aim_ref, bre_ref, bim_ref, rre_ref, rim_ref, sre_ref, sim_ref, *rest):
    nre_ref, nim_ref, y_ref = rest[-3:]
    block, channels = u_ref.shape[0], u_ref.shape[1]
    states = are_ref.shape[1]
    cut = 4

    def body(step, carry):
        first = step * many
        for p in range(0, states, 8):
            rows = slice(p, p + 8)
            a_re, a_im = are_ref[0, rows, :], aim_ref[0, rows, :]
            new_re, new_im = [], []
            for b in range(many):
                o_re, o_im = sre_ref[0, first + b, rows, :], sim_ref[0, first + b, rows, :]
                new_re.append(a_re * o_re - a_im * o_im)
                new_im.append(a_re * o_im + a_im * o_re)
            for c in range(channels):
                b_re, b_im = bre_ref[0, c, rows, :], bim_ref[0, c, rows, :]
                for b in range(many):
                    u = u_ref[first + b, c : c + 1, :]
                    new_re[b] = new_re[b] + b_re * u
                    new_im[b] = new_im[b] + b_im * u
            for b in range(many):
                nre_ref[0, first + b, rows, :] = new_re[b]
                nim_ref[0, first + b, rows, :] = new_im[b]
        for c in range(0, channels, cut):
            total = [[None] * many for _ in range(cut)]
            for p in range(0, states, 8):
                rows = slice(p, p + 8)
                h_re = [nre_ref[0, first + b, rows, :] for b in range(many)]
                h_im = [nim_ref[0, first + b, rows, :] for b in range(many)]
                for j in range(cut):
                    r_re, r_im = rre_ref[0, c + j, rows, :], rim_ref[0, c + j, rows, :]
                    for b in range(many):
                        term = r_re * h_re[b] - r_im * h_im[b]
                        total[j][b] = term if p == 0 else total[j][b] + term
            for j in range(cut):
                for b in range(many):
                    y_ref[first + b, c + j : c + j + 1, :] = jnp.sum(
                        total[j][b], axis=0, keepdims=True
                    )
        return carry

    lax.fori_loop(0, block // many, body, 0)


def state_step(layer, u, a_re, a_im, b_re, b_im, r_re, r_im, s_re, s_im, earlier):
    batch, channels, groups = u.shape
    states = a_re.shape[1]
    block = 8
    per_batch = pl.BlockSpec((block, channels, groups), lambda i: (i, 0, 0))
    eigen = pl.BlockSpec((1, states, groups), lambda i: (layer, 0, 0))
    matrix = pl.BlockSpec((1, channels, states, groups), lambda i: (layer, 0, 0, 0))
    state = pl.BlockSpec((1, block, states, groups), lambda i: (layer, i, 0, 0))
    specs = [per_batch, eigen, eigen, matrix, matrix, matrix, matrix, state, state]
    aliases = {}
    if earlier:
        aliases = {len(specs): 0, len(specs) + 1: 1}
    return pl.pallas_call(
        functools.partial(state_kernel, 4),
        grid=(batch // block,),
        out_shape=[
            jax.ShapeDtypeStruct(s_re.shape, jnp.float32),
            jax.ShapeDtypeStruct(s_im.shape, jnp.float32),
            jax.ShapeDtypeStruct(u.shape, jnp.float32),
        ],
        in_specs=specs + [ANY] * len(earlier),
        out_specs=[state, state, per_batch],
        input_output_aliases=aliases,
        name=f"state_{layer}",
    )(u, a_re, a_im, b_re, b_im, r_re, r_im, s_re, s_im, *earlier)


def on_device(
    tp,
    dp,
    tokens,
    gains,
    w_input,
    w_gating,
    w_output,
    decay_rate,
    frequency,
    log_step,
    in_real,
    in_imag,
    readout_real_matrix,
    readout_imag_matrix,
    skip_gain,
    state_real,
    state_imag,
):
    batch, width = tokens.shape
    groups, states = decay_rate.shape[1:]
    channels = groups * GS
    rows = w_input.shape[1]
    features = gains.shape[1]
    q = tp // dp
    d = lax.axis_index("dp")

    step = jnp.exp(log_step)[:, None, :]
    lam_re = -jnp.swapaxes(decay_rate, 1, 2)
    lam_im = jnp.swapaxes(frequency, 1, 2)
    magnitude = jnp.exp(lam_re * step)
    angle = lam_im * step
    abar_re = magnitude * jnp.cos(angle)
    abar_im = magnitude * jnp.sin(angle)
    denom = lam_re * lam_re + lam_im * lam_im
    num_re = abar_re - 1.0
    zoh_re = ((num_re * lam_re + abar_im * lam_im) / denom)[:, None]
    zoh_im = ((abar_im * lam_re - num_re * lam_im) / denom)[:, None]
    i_re = jnp.transpose(in_real, (0, 3, 2, 1))
    i_im = jnp.transpose(in_imag, (0, 3, 2, 1))
    bbar_re = zoh_re * i_re - zoh_im * i_im
    bbar_im = zoh_re * i_im + zoh_im * i_re
    r_re = jnp.transpose(readout_real_matrix, (0, 2, 3, 1))
    r_im = jnp.transpose(readout_imag_matrix, (0, 2, 3, 1))
    s_re = jnp.swapaxes(state_real, 2, 3)
    s_im = jnp.swapaxes(state_imag, 2, 3)
    my_gains = lax.dynamic_slice_in_dim(gains, d * rows, rows, 1).reshape(LAYERS, q, 1, width)

    shard = tokens
    news = ()
    for layer in range(LAYERS):
        got = gather(shard, tp, dp, 3 * layer + 1).reshape(q, dp * batch, width)
        xf = got.astype(jnp.float32)
        squares = jnp.sum(xf * xf, axis=(0, 2))
        scaled = (xf * my_gains[layer]).astype(jnp.bfloat16)
        if q <= 2:
            scaled = jnp.concatenate([scaled[h] for h in range(q)], axis=1)
        else:
            scaled = jnp.swapaxes(scaled, 0, 1).reshape(dp * batch, rows)
        drive = jnp.dot(scaled, w_input[layer], preferred_element_type=jnp.float32)
        gate = jnp.dot(scaled, w_gating[layer], preferred_element_type=jnp.float32)
        drive, gate, squares = exchange(
            [
                drive.astype(jnp.bfloat16).reshape(dp, batch, channels),
                gate.astype(jnp.bfloat16).reshape(dp, batch, channels),
                jnp.broadcast_to(squares.reshape(dp, batch, 1), (dp, batch, 128)),
            ],
            "dp",
            dp,
            3 * layer + 2,
        )
        meansq = jnp.sum(squares, axis=0)[:, :1] / features
        inverse = lax.rsqrt(meansq + 1e-06)
        drive = jnp.sum(drive.astype(jnp.float32), axis=0) * inverse
        gate = jnp.sum(gate.astype(jnp.float32), axis=0) * inverse
        u = jnp.swapaxes(drive.reshape(batch, groups, GS), 1, 2)
        n_re, n_im, y = state_step(
            layer, u, abar_re, abar_im, bbar_re, bbar_im, r_re, r_im, s_re, s_im, news
        )
        news = (n_re, n_im)
        y = jnp.swapaxes(y, 1, 2).reshape(batch, channels) + skip_gain[layer][None] * drive
        z = (jax.nn.gelu(y) * jax.nn.sigmoid(gate)).astype(jnp.bfloat16)
        branch = jnp.dot(z, w_output[layer], preferred_element_type=jnp.float32)
        pieces = jnp.swapaxes(branch.astype(jnp.bfloat16).reshape(batch, tp, width), 0, 1)
        (pieces,) = exchange([pieces], "tp", tp, 3 * layer + 3)
        summed = jnp.sum(pieces.astype(jnp.float32), axis=0)
        shard = (shard.astype(jnp.float32) + summed).astype(jnp.bfloat16)
    return shard, jnp.swapaxes(news[0], 2, 3), jnp.swapaxes(news[1], 2, 3)


def solution(mesh):
    placed = (
        P("dp", "tp"),
        P(),
        P(None, "dp", "tp"),
        P(None, "dp", "tp"),
        P(None, "tp", None),
        P(None, "tp", None),
        P(None, "tp", None),
        P(None, "tp"),
        P(None, "tp", None, None),
        P(None, "tp", None, None),
        P(None, "tp", None, None),
        P(None, "tp", None, None),
        P(None, "tp"),
        P(None, "dp", "tp", None),
        P(None, "dp", "tp", None),
    )
    return jax.shard_map(
        functools.partial(on_device, mesh.shape["tp"], mesh.shape["dp"]),
        mesh=mesh,
        in_specs=placed,
        out_specs=(P("dp", "tp"), P(None, "dp", "tp", None), P(None, "dp", "tp", None)),
        check_vma=False,
    )
```

profile of v0, /device:TPU:15, one launch (start us, length us, event | category | flops | bytes accessed | tf_op | source)
XLA Modules:
  0.0 234.0 jit_solution(16361997349156199498)
XLA Ops:
  0.6 0.7 exp.14
  1.3 0.8 slice_reduce_fusion
  2.1 0.9 dynamic-slice_reduce_fusion
  3.1 0.1 mul.235
  3.1 0.1 mul.201
  3.2 0.1 mul.242
  3.4 0.1 mul.226
  3.5 1.8 fusion.59
  5.4 22.5 %gather_1.1 = bf16[8,48,1056]{2,1,0:T(8,128)(2,1)} custom-call(bf16[48,1056]{1,0:T(8,128)(2,1)} %x_ref.1), custom_call_target="tpu_custom_call" | custom-call | tf_op jit(solution)/shard_map/gather_1/pallas_call | solution.py:127
  27.9 1.4 multiply_reduce_fusion.1
  29.3 0.1 reduce_sum.113
  29.4 0.1 broadcast_in_dim.8
  29.5 0.7 broadcast_in_dim.18.refs_2_
  30.3 1.3 convert_element_type.112
  31.5 0.1 fusion.37
  31.7 5.3 %fusion.27 = bf16[192,1536]{1,0:T(8,128)(2,1)} fusion(bf16[2,2112,1536]{2,1,0:T(8,128)(2,1)} %param.18, bf16[192,1056]{1,0:T(8,128)(2,1)S(1)} %get-tuple-element.36, bf16[192,1056]{1,0:T(8,128)(2,1)S(1)} %get-tuple-element.35), kind=kOutput, calls=%fused_computation.21 | convolution fusion | flops 1247625216 | bytes 7888896 | tf_op jit(solution)/shard_map/dot_general | solution.py:271
  37.1 1.3 copy-done.4
  38.4 2.4 %fusion.24 = bf16[192,1536]{1,0:T(8,128)(2,1)} fusion(bf16[2,2112,1536]{2,1,0:T(8,128)(2,1)S(1)} %copy-done.4, bf16[192,1056]{1,0:T(8,128)(2,1)S(1)} %get-tuple-element.36, bf16[192,1056]{1,0:T(8,128)(2,1)S(1)} %get-tuple-element.35), kind=kOutput, calls=%fused_computation.20 | convolution fusion | flops 1247625216 | bytes 7962624 | tf_op jit(solution)/shard_map/dot_general | solution.py:270
  40.8 21.0 %exchange_dp_2.1 = (bf16[4,48,1536]{2,1,0:T(8,128)(2,1)}, bf16[4,48,1536]{2,1,0:T(8,128)(2,1)}, f32[4,48,128]{2,1,0:T(8,128)}) custom-call(bf16[4,48,1536]{2,1,0:T(8,128)(2,1)} %bitcast.178, bf16[4,48,1536]{2,1,0:T(8,128)(2,1)} %bitcast.177, f32[4,48,128]{2,1,0:T(8,128)} %broadcast_in_dim.18.refs_2_), custom_call_target="tpu_custom_call" | custom-call | tf_op jit(solution)/shard_map/exchange_dp_2/pallas_call | solution.py:62
  61.8 1.5 convert_reduce_fusion.4
  63.3 0.1 fusion.68
  63.4 0.3 copy.73
  63.7 0.4 copy.74
  64.2 0.3 copy.68
  64.4 0.4 copy.69
  64.9 0.9 multiply_bitcast_fusion.1.u_ref
  65.7 3.2 %fusion.39 = (f32[2,16,64,96]{3,2,1,0:T(8,128)}, f32[2,16,64,96]{3,2,1,0:T(8,128)}) fusion(f32[2,96,64,16]{1,3,2,0:T(8,128)S(1)} %copy-done, f32[2,96,64,16]{1,3,2,0:T(8,128)} %param.23, f32[2,64,96]{2,1,0:T(8,128)S(1)} %get-tuple-element.39, f32[2,64,96]{2,1,0:T(8,128)S(1)} %get-tuple-element.37), kind=kLoop, calls=%fused_computation.39 | loop fusion | flops 1179648 | bytes 3244032 | tf_op jit(solution)/shard_map/add | solution.py:252
  69.0 10.5 %state_0.1 = (f32[2,48,64,96]{3,2,1,0:T(8,128)}, f32[2,48,64,96]{3,2,1,0:T(8,128)}, f32[48,16,96]{2,1,0:T(8,128)}) custom-call(f32[48,16,96]{2,1,0:T(8,128)} %multiply_bitcast_fusion.1.u_ref, f32[2,64,96]{2,1,0:T(8,128)} %get-tuple-element.40.are_ref, f32[2,64,96]{2,1,0:T(8,128)} %get-tuple-element.38.aim_ref, f32[2,16,64,96]{3,2,1,0:T(8,128)} %get-tuple-element.32.bre_ref, ...), custom_call_target="tpu_custom_call" | custom-call | tf_op jit(solution)/shard_map/state_0/pallas_call | solution.py:196
  79.5 1.3 fusion.48
  80.8 0.4 copy.75
  81.2 10.9 %fusion.6 = bf16[48,8448]{1,0:T(8,128)(2,1)S(1)} fusion(bf16[48,1536]{0,1:T(8,128)(2,1)S(1)} %bitcast.175, bf16[2,1536,8448]{2,1,0:T(8,128)(2,1)} %param.19), kind=kOutput, calls=%fused_computation.6 | convolution fusion | flops 1246113792 | bytes 26910720 | tf_op jit(solution)/shard_map/dot_general | solution.py:293
  92.1 1.5 reshape.100
  93.6 1.0 copy.91
  94.6 23.4 %exchange_tp_3.1 = bf16[8,48,1056]{2,1,0:T(8,128)(2,1)} custom-call(bf16[8,48,1056]{2,1,0:T(8,128)(2,1)} %bitcast.167), custom_call_target="tpu_custom_call" | custom-call | tf_op jit(solution)/shard_map/exchange_tp_3/pallas_call | solution.py:62
  118.0 1.3 convert_reduce_fusion.1
  119.3 0.7 add_convert_fusion.1.x_ref
  120.0 22.7 %gather_4.1 = bf16[8,48,1056]{2,1,0:T(8,128)(2,1)} custom-call(bf16[48,1056]{1,0:T(8,128)(2,1)} %add_convert_fusion.1.x_ref), custom_call_target="tpu_custom_call" | custom-call | tf_op jit(solution)/shard_map/gather_4/pallas_call | solution.py:127
  142.7 1.4 multiply_reduce_fusion
  144.2 0.1 reduce_sum.122
  144.3 0.1 broadcast_in_dim.19
  144.4 0.7 broadcast_in_dim.20.refs_2_
  145.1 1.3 convert_element_type.113
  146.4 0.1 fusion.36
  146.6 5.2 %fusion.33 = bf16[192,1536]{1,0:T(8,128)(2,1)} fusion(bf16[2,2112,1536]{2,1,0:T(8,128)(2,1)} %param.18, bf16[192,1056]{1,0:T(8,128)(2,1)S(1)} %get-tuple-element.34, bf16[192,1056]{1,0:T(8,128)(2,1)S(1)} %get-tuple-element.33), kind=kOutput, calls=%fused_computation.23 | convolution fusion | flops 1247625216 | bytes 7888896 | tf_op jit(solution)/shard_map/dot_general | solution.py:271
  151.8 5.2 %fusion.30 = bf16[192,1536]{1,0:T(8,128)(2,1)} fusion(bf16[2,2112,1536]{2,1,0:T(8,128)(2,1)} %param.17, bf16[192,1056]{1,0:T(8,128)(2,1)S(1)} %get-tuple-element.34, bf16[192,1056]{1,0:T(8,128)(2,1)S(1)} %get-tuple-element.33), kind=kOutput, calls=%fused_computation.22 | convolution fusion | flops 1247625216 | bytes 7888896 | tf_op jit(solution)/shard_map/dot_general | solution.py:270
  157.0 20.6 %exchange_dp_5.1 = (bf16[4,48,1536]{2,1,0:T(8,128)(2,1)}, bf16[4,48,1536]{2,1,0:T(8,128)(2,1)}, f32[4,48,128]{2,1,0:T(8,128)}) custom-call(bf16[4,48,1536]{2,1,0:T(8,128)(2,1)} %bitcast.180, bf16[4,48,1536]{2,1,0:T(8,128)(2,1)} %bitcast.179, f32[4,48,128]{2,1,0:T(8,128)} %broadcast_in_dim.20.refs_2_), custom_call_target="tpu_custom_call" | custom-call | tf_op jit(solution)/shard_map/exchange_dp_5/pallas_call | solution.py:62
  177.6 1.2 convert_reduce_fusion.3
  178.8 0.9 reduce_sum.126
  179.7 0.1 fusion.65
  179.8 1.2 convert_reduce_fusion.2
  181.0 0.3 copy.80
  181.3 0.4 copy.81
  181.7 0.3 copy.77
  182.0 0.4 copy.78
  182.4 0.9 multiply_bitcast_fusion.u_ref
  183.3 10.4 %state_1.1 = (f32[2,48,64,96]{3,2,1,0:T(8,128)}, f32[2,48,64,96]{3,2,1,0:T(8,128)}, f32[48,16,96]{2,1,0:T(8,128)}) custom-call(f32[48,16,96]{2,1,0:T(8,128)} %multiply_bitcast_fusion.u_ref, f32[2,64,96]{2,1,0:T(8,128)} %get-tuple-element.40.are_ref, f32[2,64,96]{2,1,0:T(8,128)} %get-tuple-element.38.aim_ref, ...), custom_call_target="tpu_custom_call", output_to_operand_aliasing={{0}: (9, {}), {1}: (10, {})} | custom-call | tf_op jit(solution)/shard_map/state_1/pallas_call | solution.py:196
  193.7 1.3 fusion.57
  195.0 0.4 copy.82
  195.4 11.1 %fusion.9 = bf16[48,8448]{1,0:T(8,128)(2,1)S(1)} fusion(bf16[48,1536]{0,1:T(8,128)(2,1)S(1)} %bitcast.176, bf16[2,1536,8448]{2,1,0:T(8,128)(2,1)} %param.19), kind=kOutput, calls=%fused_computation.7 | convolution fusion | flops 1246113792 | bytes 26910720 | tf_op jit(solution)/shard_map/dot_general | solution.py:293
  206.5 1.5 reshape.103
  208.0 1.0 copy.90
  209.0 22.9 %exchange_tp_6.1 = bf16[8,48,1056]{2,1,0:T(8,128)(2,1)} custom-call(bf16[8,48,1056]{2,1,0:T(8,128)(2,1)} %bitcast.168), custom_call_target="tpu_custom_call" | custom-call | tf_op jit(solution)/shard_map/exchange_tp_6/pallas_call | solution.py:62
  232.0 1.3 convert_reduce_fusion
  233.3 0.7 add_convert_fusion
  (16 shorter events, 0.3 us)
Async XLA Ops:
  31.7 6.8 %copy-start.4 = (bf16[2,2112,1536]{2,1,0:T(8,128)(2,1)S(1)}, bf16[2,2112,1536]{2,1,0:T(8,128)(2,1)}, u32[]{:S(2)}) copy-start(bf16[2,2112,1536]{2,1,0:T(8,128)(2,1)} %param.17) | copy-start | bytes 38928388
  61.8 1.5 copy-start.3
  64.1 1.6 copy-start
  94.6 24.8 %copy-start.2 = (bf16[48,1056]{1,0:T(8,128)(2,1)S(1)}, bf16[48,1056]{1,0:T(8,128)(2,1)}, u32[]{:S(2)}) copy-start(bf16[48,1056]{1,0:T(8,128)(2,1)} %x_ref.1) | copy-start | bytes 304132
  209.0 24.3 %copy-start.1 = (bf16[48,1056]{1,0:T(8,128)(2,1)S(1)}, bf16[48,1056]{1,0:T(8,128)(2,1)}, u32[]{:S(2)}) copy-start(bf16[48,1056]{1,0:T(8,128)(2,1)} %add_convert_fusion.1.x_ref) | copy-start | bytes 304132
where the time goes:
time: 235 us; the launch traced here: 234 us
  Pallas kernels  154 us (66%)
  matrix products  40.1 us (17%)
  other arithmetic  24 us (10%)
  local copies, waits for them, and re-layouts  14.7 us (6%)
    pallas_call x4, Pallas kernels, exchange(): pl.pallas_call(functools.partial(exchange_kernel, axis, n, count), out_sh...  88 us
    pallas_call x2, Pallas kernels, gather(): pl.pallas_call(functools.partial(gather_kernel, tp, dp), out_shape=jax.Sh...  45.3 us
    dot_general x2, matrix products, on_device(): branch = jnp.dot(z, w_output[layer], preferred_element_type=jnp.float32)  22 us
    pallas_call x2, Pallas kernels, state_step(): pl.pallas_call(functools.partial(state_kernel, 4), grid=(batch // block,)...  20.9 us
    dot_general x2, matrix products, on_device(): gate = jnp.dot(scaled, w_gating[layer], preferred_element_type=jnp.float32)  10.6 us
    dot_general x2, matrix products, on_device(): drive = jnp.dot(scaled, w_input[layer], preferred_element_type=jnp.float32)  7.55 us
    reshape x4, local copies, waits for them, and re-layouts, on_device(): branch.astype(jnp.bfloat16).reshape(batch, tp, width)  5.01 us

commit v1 on v0

--- a/solution.py
+++ b/solution.py
@@ -208,6 +208,397 @@
     )(u, a_re, a_im, b_re, b_im, r_re, r_im, s_re, s_im, *earlier)
 
 
+def remote(src, dst, send, recv, target):
+    return pltpu.make_async_remote_copy(
+        src_ref=src,
+        dst_ref=dst,
+        send_sem=send,
+        recv_sem=recv,
+        device_id=target,
+        device_id_type=MESH,
+    )
+
+
+def greet(barrier, target):
+    pl.semaphore_signal(barrier, inc=1, device_id=target, device_id_type=MESH)
+
+
+def project_kernel(
+    layer, tp, dp, features,
+    x_ref, gain_ref, win_ref, wgate_ref, drive_ref, gate_ref,
+    xg, wbuf, scaled, acc, squares,
+    out1, in1, out2, in2, sq_out1, sq_in1, sq_out2, sq_in2,
+    wsem, gsend, grecv, ysend, yrecv, send1, recv1, send2, recv2,
+):
+    q = tp // dp
+    half = dp // 2
+    t, d = lax.axis_index("tp"), lax.axis_index("dp")
+    z, y = t // q, t % q
+    x, c = d // 2, d % 2
+    home = z == d
+    batch, width = x_ref.shape
+    channels = drive_ref.shape[1]
+    partner = 2 * x + 1 - c
+    far = (d + 2) % dp
+    beside = 2 * (far // 2) + 1 - far % 2
+    other = 1 - y
+
+    weights = []
+    for m, w in enumerate((win_ref, wgate_ref)):
+        for h in range(q):
+            copy = pltpu.make_async_copy(
+                w.at[layer, pl.ds(h * width, width), :], wbuf.at[m, h], wsem.at[m, h]
+            )
+            copy.start()
+
+    barrier = pltpu.get_barrier_semaphore()
+    for e in range(dp):
+        @pl.when(jnp.logical_not(jnp.logical_and(home, d == e)))
+        def _():
+            greet(barrier, {"tp": d * q + y, "dp": e})
+    greet(barrier, {"tp": z * q + other})
+    greet(barrier, {"dp": partner})
+    greet(barrier, {"dp": far})
+    pl.semaphore_wait(barrier, dp + 3 - home.astype(jnp.int32))
+
+    upper = z // half
+    order = [
+        (dp - 1) * (1 - upper),
+        half - upper,
+        z + 1 - 2 * (z % 2),
+        z,
+    ]
+
+    def spread(i):
+        return remote(
+            x_ref, xg.at[y, d], gsend.at[i], grecv.at[d], {"tp": order[i] * q + y, "dp": z}
+        )
+
+    for i in range(dp - 1):
+        spread(i).start()
+
+    @pl.when(home)
+    def _():
+        xg[y, d] = x_ref[...]
+
+    @pl.when(jnp.logical_not(home))
+    def _():
+        spread(dp - 1).start()
+
+    def across(src, e, slot):
+        return remote(
+            src, xg.at[slot, e], ysend.at[e], yrecv.at[e], {"tp": z * q + other}
+        )
+
+    slots = [d, partner, far, beside]
+    for i in range(dp):
+        e = slots[i]
+        if i == 0:
+            @pl.when(home)
+            def _():
+                across(x_ref, e, y).start()
+
+            @pl.when(jnp.logical_not(home))
+            def _():
+                remote(x_ref, xg.at[y, e], gsend.at[0], grecv.at[e], {"dp": partner}).wait_recv()
+                across(xg.at[y, e], e, y).start()
+        else:
+            remote(x_ref, xg.at[y, e], gsend.at[0], grecv.at[e], {"dp": partner}).wait_recv()
+            across(xg.at[y, e], e, y).start()
+
+    def scale(h, first):
+        gain = gain_ref[h]
+        for e in range(dp):
+            xf = xg[h, e].astype(jnp.float32)
+            total = jnp.broadcast_to(jnp.sum(xf * xf, axis=1, keepdims=True), squares.shape[1:])
+            squares[e] = total if first else squares[e] + total
+            scaled[e * batch : (e + 1) * batch, :] = (xf * gain).astype(jnp.bfloat16)
+
+    cut = 256
+
+    scale(y, True)
+    for m in range(2):
+        pltpu.make_async_copy(
+            win_ref.at[layer, pl.ds(0, width), :], wbuf.at[m, y], wsem.at[m, y]
+        ).wait()
+
+        def first(n, carry):
+            cols = pl.ds(pl.multiple_of(n * cut, cut), cut)
+            part = jnp.dot(scaled[...], wbuf[m, y, :, cols], preferred_element_type=jnp.float32)
+            acc[m, :, :, cols] = part.reshape(dp, batch, cut)
+            return carry
+
+        lax.fori_loop(0, channels // cut, first, 0)
+
+    for i in range(dp):
+        e = slots[i]
+        across(x_ref, e, other).wait_recv()
+    scale(other, False)
+    for h in range(half):
+        sq_out1[h] = squares[2 * h + 1 - c]
+    remote(sq_out1, sq_in1, send1.at[2], recv1.at[2], {"dp": partner}).start()
+
+    def stage1(m):
+        return remote(out1.at[m], in1.at[m], send1.at[m], recv1.at[m], {"dp": partner})
+
+    def stage2(m):
+        return remote(out2.at[m], in2.at[m], send2.at[m], recv2.at[m], {"dp": far})
+
+    for m in range(2):
+        pltpu.make_async_copy(
+            win_ref.at[layer, pl.ds(0, width), :], wbuf.at[m, other], wsem.at[m, other]
+        ).wait()
+
+        def second(n, carry):
+            cols = pl.ds(pl.multiple_of(n * cut, cut), cut)
+            part = jnp.dot(
+                scaled[...], wbuf[m, other, :, cols], preferred_element_type=jnp.float32
+            )
+            acc[m, :, :, cols] = acc[m, :, :, cols] + part.reshape(dp, batch, cut)
+            for h in range(half):
+                out1[m, h, :, cols] = acc[m, 2 * h + 1 - c, :, cols].astype(jnp.bfloat16)
+            return carry
+
+        lax.fori_loop(0, channels // cut, second, 0)
+        stage1(m).start()
+
+    remote(sq_out1, sq_in1, send1.at[2], recv1.at[2], {"dp": partner}).wait()
+    sq_out2[...] = squares[far] + sq_in1[1 - x]
+    sq2 = remote(sq_out2, sq_in2, send2.at[2], recv2.at[2], {"dp": far})
+    sq2.start()
+    for m in range(2):
+        stage1(m).wait()
+        out2[m] = (acc[m, far] + in1[m, 1 - x].astype(jnp.float32)).astype(jnp.bfloat16)
+        stage2(m).start()
+        acc[m, d] = acc[m, d] + in1[m, x].astype(jnp.float32)
+    sq2.wait()
+    meansq = (squares[d] + sq_in1[x] + sq_in2[...])[:, :1] / features
+    inverse = lax.rsqrt(meansq + 1e-06)
+    for m, result in enumerate((drive_ref, gate_ref)):
+        stage2(m).wait()
+        result[...] = (acc[m, d] + in2[m].astype(jnp.float32)) * inverse
+
+    for i in range(dp - 1):
+        spread(i).wait_send()
+
+    @pl.when(jnp.logical_not(home))
+    def _():
+        spread(dp - 1).wait_send()
+
+    for i in range(dp):
+        across(x_ref, slots[i], y).wait_send()
+
+
+def project(layer, x, gain, w_input, w_gating, tp, dp, features, ident):
+    batch, width = x.shape
+    channels = w_input.shape[2]
+    q = tp // dp
+    half = dp // 2
+    bf, f32 = jnp.bfloat16, jnp.float32
+    vmem = pl.BlockSpec(memory_space=pltpu.VMEM)
+    dma = pltpu.SemaphoreType.DMA
+    return pl.pallas_call(
+        functools.partial(project_kernel, layer, tp, dp, features),
+        out_shape=[jax.ShapeDtypeStruct((batch, channels), f32)] * 2,
+        in_specs=[vmem, vmem, ANY, ANY],
+        out_specs=[vmem, vmem],
+        scratch_shapes=[
+            pltpu.VMEM((q, dp, batch, width), bf),
+            pltpu.VMEM((2, q, width, channels), bf),
+            pltpu.VMEM((dp * batch, width), bf),
+            pltpu.VMEM((2, dp, batch, channels), f32),
+            pltpu.VMEM((dp, batch, 128), f32),
+            pltpu.VMEM((2, half, batch, channels), bf),
+            pltpu.VMEM((2, half, batch, channels), bf),
+            pltpu.VMEM((2, batch, channels), bf),
+            pltpu.VMEM((2, batch, channels), bf),
+            pltpu.VMEM((half, batch, 128), f32),
+            pltpu.VMEM((half, batch, 128), f32),
+            pltpu.VMEM((batch, 128), f32),
+            pltpu.VMEM((batch, 128), f32),
+            dma((2, q)),
+            dma((dp,)),
+            dma((dp,)),
+            dma((dp,)),
+            dma((dp,)),
+            dma((3,)),
+            dma((3,)),
+            dma((3,)),
+            dma((3,)),
+        ],
+        compiler_params=pltpu.CompilerParams(
+            collective_id=ident, has_side_effects=True, vmem_limit_bytes=62 * 2**20
+        ),
+        name=f"project_{layer}",
+    )(x, gain, w_input, w_gating)
+
+
+def merge_kernel(
+    layer, tp, dp,
+    z_ref, x_ref, w_ref, out_ref,
+    both, wbuf, prod, blocks, ybuf, yin, zbuf, zin, own, last, last_in,
+    wsem, psend, precv, ysend, yrecv, zsend, zrecv, fsend, frecv,
+):
+    q = tp // dp
+    half = dp // 2
+    t, d = lax.axis_index("tp"), lax.axis_index("dp")
+    z, y = t // q, t % q
+    x, c = d // 2, d % 2
+    partner = 2 * x + 1 - c
+    other = 1 - y
+    batch, width = x_ref.shape
+    columns = wbuf.shape[1]
+    pieces = 3
+    piece = columns // pieces
+    collects = z // half == c
+
+    def fetch(n):
+        return pltpu.make_async_copy(
+            w_ref.at[layer, :, pl.ds(pl.multiple_of(c * columns + n * piece, 128), piece)],
+            wbuf.at[:, pl.ds(n * piece, piece)],
+            wsem.at[n],
+        )
+
+    for n in range(pieces):
+        fetch(n).start()
+
+    barrier = pltpu.get_barrier_semaphore()
+    greet(barrier, {"dp": partner})
+    greet(barrier, {"tp": z * q + other})
+
+    @pl.when(collects)
+    def _():
+        for o in range(1, dp):
+            greet(barrier, {"tp": ((z + o) % dp) * q + y})
+
+    pl.semaphore_wait(barrier, 2 + half - collects.astype(jnp.int32))
+
+    swap = remote(z_ref, both.at[c], psend, precv, {"dp": partner})
+    swap.start()
+    both[c] = z_ref[...]
+    remote(z_ref, both.at[1 - c], psend, precv, {"dp": partner}).wait_recv()
+    rows = both[...].reshape(2 * batch, both.shape[2])
+    for n in range(pieces):
+        fetch(n).wait()
+        span = slice(n * piece, (n + 1) * piece)
+        prod[:, span] = jnp.dot(rows, wbuf[:, span], preferred_element_type=jnp.float32)
+    for j in range(half * q):
+        for e in range(2):
+            blocks[j, e] = prod[e * batch : (e + 1) * batch, j * width : (j + 1) * width]
+
+    first = jnp.where(c == 0, jnp.where(z == 0, 1, 0), jnp.where(z == dp - 1, 0, 1))
+    turns = [first, 1 - first]
+
+    def over_y(k, e):
+        return remote(
+            ybuf.at[k, e], yin.at[k, e], ysend.at[k, e], yrecv.at[k, e], {"tp": z * q + other}
+        )
+
+    def over_z(k, e):
+        return remote(
+            zbuf.at[k, e],
+            zin.at[z, e],
+            zsend.at[k, e],
+            zrecv.at[z, e],
+            {"tp": (half * c + k) * q + y},
+        )
+
+    for k in turns:
+        for e in range(2):
+            ybuf[k, e] = blocks[q * k + other, e].astype(jnp.bfloat16)
+            over_y(k, e).start()
+    for k in turns:
+        mine = half * c + k == z
+        for e in range(2):
+            over_y(k, e).wait_recv()
+            total = blocks[q * k + y, e] + yin[k, e].astype(jnp.float32)
+
+            @pl.when(mine)
+            def _():
+                own[e] = total
+
+            @pl.when(jnp.logical_not(mine))
+            def _():
+                zbuf[k, e] = total.astype(jnp.bfloat16)
+                over_z(k, e).start()
+
+    final = remote(last, last_in, fsend, frecv, {"dp": partner})
+
+    def gathered(e):
+        total = own[e]
+        for o in range(1, dp):
+            source = (z + o) % dp
+            remote(
+                zbuf.at[0, 0], zin.at[source, e], zsend.at[0, 0], zrecv.at[source, e],
+                {"dp": partner},
+            ).wait_recv()
+            total = total + zin[source, e].astype(jnp.float32)
+        return total
+
+    @pl.when(collects)
+    def _():
+        last[...] = gathered(1 - c)
+        final.start()
+        out_ref[...] = (x_ref[...].astype(jnp.float32) + gathered(c)).astype(jnp.bfloat16)
+        final.wait_send()
+
+    @pl.when(jnp.logical_not(collects))
+    def _():
+        final.wait_recv()
+        out_ref[...] = (x_ref[...].astype(jnp.float32) + last_in[...]).astype(jnp.bfloat16)
+
+    swap.wait_send()
+    for k in range(2):
+        for e in range(2):
+            over_y(k, e).wait_send()
+
+            @pl.when(half * c + k != z)
+            def _():
+                over_z(k, e).wait_send()
+
+
+def merge(layer, gated, x, w_output, tp, dp, ident):
+    batch, width = x.shape
+    channels, features = w_output.shape[1:]
+    q = tp // dp
+    half = dp // 2
+    bf, f32 = jnp.bfloat16, jnp.float32
+    vmem = pl.BlockSpec(memory_space=pltpu.VMEM)
+    dma = pltpu.SemaphoreType.DMA
+    return pl.pallas_call(
+        functools.partial(merge_kernel, layer, tp, dp),
+        out_shape=jax.ShapeDtypeStruct((batch, width), bf),
+        in_specs=[vmem, vmem, ANY],
+        out_specs=vmem,
+        scratch_shapes=[
+            pltpu.VMEM((2, batch, channels), bf),
+            pltpu.VMEM((channels, features // 2), bf),
+            pltpu.VMEM((2 * batch, features // 2), f32),
+            pltpu.VMEM((half * q, 2, batch, width), f32),
+            pltpu.VMEM((half, 2, batch, width), bf),
+            pltpu.VMEM((half, 2, batch, width), bf),
+            pltpu.VMEM((half, 2, batch, width), bf),
+            pltpu.VMEM((dp, 2, batch, width), bf),
+            pltpu.VMEM((2, batch, width), f32),
+            pltpu.VMEM((batch, width), f32),
+            pltpu.VMEM((batch, width), f32),
+            dma((3,)),
+            dma,
+            dma,
+            dma((half, 2)),
+            dma((half, 2)),
+            dma((half, 2)),
+            dma((dp, 2)),
+            dma,
+            dma,
+        ],
+        compiler_params=pltpu.CompilerParams(
+            collective_id=ident, has_side_effects=True, vmem_limit_bytes=62 * 2**20
+        ),
+        name=f"merge_{layer}",
+    )(gated, x, w_output)
+
+
 def on_device(
     tp,
     dp,
@@ -258,7 +649,21 @@
 
     shard = tokens
     news = ()
+    paired = q == 2 and dp == 4
     for layer in range(LAYERS):
+        if paired:
+            drive, gate = project(
+                layer, shard, my_gains[layer], w_input, w_gating, tp, dp, features, 2 * layer + 1
+            )
+            u = jnp.swapaxes(drive.reshape(batch, groups, GS), 1, 2)
+            n_re, n_im, y = state_step(
+                layer, u, abar_re, abar_im, bbar_re, bbar_im, r_re, r_im, s_re, s_im, news
+            )
+            news = (n_re, n_im)
+            y = jnp.swapaxes(y, 1, 2).reshape(batch, channels) + skip_gain[layer][None] * drive
+            z = (jax.nn.gelu(y) * jax.nn.sigmoid(gate)).astype(jnp.bfloat16)
+            shard = merge(layer, z, shard, w_output, tp, dp, 2 * layer + 2)
+            continue
         got = gather(shard, tp, dp, 3 * layer + 1).reshape(q, dp * batch, width)
         xf = got.astype(jnp.float32)
         squares = jnp.sum(xf * xf, axis=(0, 2))

time: 235 us -> 163 us (0.69)
  matrix products: 40.1 us -> 0 us
  other arithmetic: 24 us -> 6.68 us
  Pallas kernels: 154 us -> 142 us
    dot_general x6 -> x0, matrix products: 40.1 us -> none  [the longest x2 22 us: on_device(): branch = jnp.dot(z, w_output[layer], preferred_element_type=jnp.float32)]
    pallas_call x6 -> x4, Pallas kernels: 133 us -> 121 us  [the longest x2 62.5 us: project(): pl.pallas_call(functools.partial(project_kernel, layer, tp, dp, features)...]
    reduce_sum x11 -> x0, other arithmetic: 10.3 us -> none  [the longest x4 2.89 us: on_device(): squares = jnp.sum(xf * xf, axis=(0, 2))]
    convert_element_type x6 -> x0, other arithmetic: 4.13 us -> none  [the longest x2 2.56 us: on_device(): xf = got.astype(jnp.float32)]
    reduce_sum x10 -> x0, local copies, waits for them, and re-layouts: 2.93 us -> none  [the longest x4 1.39 us: on_device(): gate = jnp.sum(gate.astype(jnp.float32), axis=0) * inverse]
    transpose x0 -> x2, local copies, waits for them, and re-layouts: none -> 2.83 us  [on_device(): jnp.swapaxes(y, 1, 2).reshape(batch, channels)]
    pallas_call x0 -> x2, local copies, waits for them, and re-layouts: none -> 2.45 us  [project(): pl.pallas_call(functools.partial(project_kernel, layer, tp, dp, features)...]
where the time goes in v1:
time: 163 us
  Pallas kernels  142 us (87%)
  local copies, waits for them, and re-layouts  13.4 us (8%)
  other arithmetic  6.68 us (4%)
    pallas_call x2, Pallas kernels, project(): pl.pallas_call(functools.partial(project_kernel, layer, tp, dp, features)...  62.5 us
    pallas_call x2, Pallas kernels, merge(): pl.pallas_call(functools.partial(merge_kernel, layer, tp, dp), out_shape=...  58.5 us
    pallas_call x2, Pallas kernels, state_step(): pl.pallas_call(functools.partial(state_kernel, 4), grid=(batch // block,)...  20.9 us

profile of v1, /device:TPU:15, one launch (start us, length us, event | category | flops | bytes accessed | tf_op | source)
XLA Modules:
  0.0 162.7 jit_solution(12560809653646915780)
XLA Ops:
  0.6 0.7 exp.12
  1.3 0.8 slice_reduce_fusion
  2.1 0.9 dynamic-slice_reduce_fusion
  3.1 0.7 squeeze.7.gain_ref
  3.7 0.7 squeeze.6.gain_ref
  4.4 1.8 %fusion.21 = (f32[2,64,96]{2,1,0:T(8,128)S(1)}, f32[2,64,96]{2,1,0:T(8,128)}, f32[2,64,96]{2,1,0:T(8,128)S(1)}, f32[2,64,96]{2,1,0:T(8,128)}) fusion(f32[2,96,64]{1,2,0:T(8,128)} %param.21, f32[2,96,64]{1,2,0:T(8,128)} %param.20, f32[2,96]{1,0:T(2,128)S(1)} %exp.12), kind=kLoop, calls=%fused_computation.32 | loop fusion | flops 208896 | bytes 295680 | tf_op jit(solution)/shard_map/div | solution.py:638
  6.2 0.0 copy-start.2
  6.2 32.3 %project_0.1 = (f32[48,1536]{1,0:T(8,128)}, f32[48,1536]{1,0:T(8,128)}) custom-call(bf16[48,1056]{1,0:T(8,128)(2,1)} %x_ref.3, f32[2,1,1056]{2,1,0:T(1,128)} %squeeze.6.gain_ref, bf16[2,2112,1536]{2,1,0:T(8,128)(2,1)} %win_ref.3, bf16[2,2112,1536]{2,1,0:T(8,128)(2,1)} %wgate_ref.3), custom_call_target="tpu_custom_call" | custom-call | tf_op jit(solution)/shard_map/project_0/pallas_call | solution.py:400
  38.6 1.2 copy.24
  39.8 1.2 copy.25
  41.0 0.0 copy-done.2
  41.0 3.2 %fusion.1 = (f32[2,16,64,96]{3,2,1,0:T(8,128)}, f32[2,16,64,96]{3,2,1,0:T(8,128)}) fusion(f32[2,96,64,16]{1,3,2,0:T(8,128)S(1)} %copy-done.2, f32[2,96,64,16]{1,3,2,0:T(8,128)} %param.23, f32[2,64,96]{2,1,0:T(8,128)S(1)} %get-tuple-element.31, f32[2,64,96]{2,1,0:T(8,128)S(1)} %get-tuple-element.29), kind=kLoop, calls=%fused_computation.3 | loop fusion | flops 1179648 | bytes 3244032 | tf_op jit(solution)/shard_map/add | solution.py:643
  44.2 0.0 copy-start
  44.2 0.0 copy-start.3
  44.2 10.5 %state_0.1 = (f32[2,48,64,96]{3,2,1,0:T(8,128)}, f32[2,48,64,96]{3,2,1,0:T(8,128)}, f32[48,16,96]{2,1,0:T(8,128)}) custom-call(f32[48,16,96]{2,1,0:T(8,128)} %bitcast.101, f32[2,64,96]{2,1,0:T(8,128)} %get-tuple-element.32.are_ref, f32[2,64,96]{2,1,0:T(8,128)} %get-tuple-element.30.aim_ref, f32[2,16,64,96]{3,2,1,0:T(8,128)} %get-tuple-element.28.bre_ref, ...), custom_call_target="tpu_custom_call" | custom-call | tf_op jit(solution)/shard_map/state_0/pallas_call | solution.py:196
  54.6 1.4 copy.28
  56.0 0.2 copy.29
  56.3 0.0 copy-done
  56.3 0.0 copy-done.3
  56.3 0.9 fusion.10.z_ref
  57.1 30.1 %merge_0.1.x_ref = bf16[48,1056]{1,0:T(8,128)(2,1)} custom-call(bf16[48,1536]{1,0:T(8,128)(2,1)} %fusion.10.z_ref, bf16[48,1056]{1,0:T(8,128)(2,1)} %x_ref.3, bf16[2,1536,8448]{2,1,0:T(8,128)(2,1)} %w_ref.3), custom_call_target="tpu_custom_call" | custom-call | tf_op jit(solution)/shard_map/merge_0/pallas_call | solution.py:568
  87.3 30.1 %project_1.1 = (f32[48,1536]{1,0:T(8,128)}, f32[48,1536]{1,0:T(8,128)}) custom-call(bf16[48,1056]{1,0:T(8,128)(2,1)} %merge_0.1.x_ref, f32[2,1,1056]{2,1,0:T(1,128)} %squeeze.7.gain_ref, bf16[2,2112,1536]{2,1,0:T(8,128)(2,1)} %win_ref.3, bf16[2,2112,1536]{2,1,0:T(8,128)(2,1)} %wgate_ref.3), custom_call_target="tpu_custom_call" | custom-call | tf_op jit(solution)/shard_map/project_1/pallas_call | solution.py:400
  117.4 1.2 copy.30
  118.6 1.2 copy.31
  119.8 0.0 copy-start.1
  119.8 0.0 copy-start.4
  119.8 10.4 %state_1.1 = (f32[2,48,64,96]{3,2,1,0:T(8,128)}, f32[2,48,64,96]{3,2,1,0:T(8,128)}, f32[48,16,96]{2,1,0:T(8,128)}) custom-call(f32[48,16,96]{2,1,0:T(8,128)} %bitcast.102, f32[2,64,96]{2,1,0:T(8,128)} %get-tuple-element.32.are_ref, f32[2,64,96]{2,1,0:T(8,128)} %get-tuple-element.30.aim_ref, ...), custom_call_target="tpu_custom_call", output_to_operand_aliasing={{0}: (9, {}), {1}: (10, {})} | custom-call | tf_op jit(solution)/shard_map/state_1/pallas_call | solution.py:196
  130.2 1.4 copy.32
  131.7 0.2 copy.33
  131.9 0.0 copy-done.1
  131.9 0.0 copy-done.4
  131.9 0.8 fusion.19.z_ref
  132.7 28.4 %merge_1.1 = bf16[48,1056]{1,0:T(8,128)(2,1)} custom-call(bf16[48,1536]{1,0:T(8,128)(2,1)} %fusion.19.z_ref, bf16[48,1056]{1,0:T(8,128)(2,1)} %merge_0.1.x_ref, bf16[2,1536,8448]{2,1,0:T(8,128)(2,1)} %w_ref.3), custom_call_target="tpu_custom_call" | custom-call | tf_op jit(solution)/shard_map/merge_1/pallas_call | solution.py:568
  161.1 1.6 copy.41
Async XLA Ops:
  6.2 34.7 %copy-start.2 = (f32[2,96,64,16]{1,3,2,0:T(8,128)S(1)}, f32[2,96,64,16]{1,3,2,0:T(8,128)}, u32[]{:S(2)}) copy-start(f32[2,96,64,16]{1,3,2,0:T(8,128)} %param.24) | copy-start | bytes 2359300
  44.2 12.1 %copy-start = (f32[48,1536]{1,0:T(8,128)S(1)}, f32[48,1536]{1,0:T(8,128)}, u32[]{:S(2)}) copy-start(f32[48,1536]{1,0:T(8,128)} %get-tuple-element.13) | copy-start | bytes 884740
  44.2 12.1 %copy-start.3 = (f32[48,1536]{1,0:T(8,128)S(1)}, f32[48,1536]{1,0:T(8,128)}, u32[]{:S(2)}) copy-start(f32[48,1536]{1,0:T(8,128)} %get-tuple-element.15) | copy-start | bytes 884740
  119.8 12.1 %copy-start.1 = (f32[48,1536]{1,0:T(8,128)S(1)}, f32[48,1536]{1,0:T(8,128)}, u32[]{:S(2)}) copy-start(f32[48,1536]{1,0:T(8,128)} %get-tuple-element.16) | copy-start | bytes 884740
  119.8 12.1 %copy-start.4 = (f32[48,1536]{1,0:T(8,128)S(1)}, f32[48,1536]{1,0:T(8,128)}, u32[]{:S(2)}) copy-start(f32[48,1536]{1,0:T(8,128)} %get-tuple-element.20) | copy-start | bytes 884740

commit v2 on v1

--- a/solution.py
+++ b/solution.py
@@ -223,13 +223,23 @@
     pl.semaphore_signal(barrier, inc=1, device_id=target, device_id_type=MESH)
 
 
-def project_kernel(
-    layer, tp, dp, features,
-    x_ref, gain_ref, win_ref, wgate_ref, drive_ref, gate_ref,
-    xg, wbuf, scaled, acc, squares,
-    out1, in1, out2, in2, sq_out1, sq_in1, sq_out2, sq_in2,
-    wsem, gsend, grecv, ysend, yrecv, send1, recv1, send2, recv2,
+def layer_kernel(
+    layer, tp, dp, features, earlier,
+    x_ref, gain_ref, skip_ref, win_ref, wgate_ref, wout_ref,
+    logstep_ref, decay_ref, freq_ref, ire_ref, iim_ref, rre_ref, rim_ref, sre_ref, sim_ref,
+    *rest,
 ):
+    out_ref, nre_ref, nim_ref = rest[earlier : earlier + 3]
+    (
+        xg, wbuf, scaled, acc, squares,
+        out1, in1, out2, in2, sq_out1, sq_in1, sq_out2, sq_in2,
+        decay, freq, i_re, i_im,
+        a_re, a_im, b_re, b_im, r_re, r_im, h_re, h_im,
+        mix, y0, y0p, y3, u3, ub, flip, flipy, unat, gated,
+        both, wobuf, prod, blocks, ybuf, yin, zbuf, zin, own, last, last_in,
+        wsem, gsend, grecv, across_send, across_recv, send1, recv1, send2, recv2,
+        ssem, osem, psem, swap_send, swap_recv, ysend, yrecv, zsend, zrecv, fsend, frecv,
+    ) = rest[earlier + 3 :]
     q = tp // dp
     half = dp // 2
     t, d = lax.axis_index("tp"), lax.axis_index("dp")
@@ -237,19 +247,35 @@
     x, c = d // 2, d % 2
     home = z == d
     batch, width = x_ref.shape
-    channels = drive_ref.shape[1]
+    channels = unat.shape[1]
+    states, groups = a_re.shape
+    gs = channels // groups
     partner = 2 * x + 1 - c
     far = (d + 2) % dp
     beside = 2 * (far // 2) + 1 - far % 2
     other = 1 - y
-
-    weights = []
-    for m, w in enumerate((win_ref, wgate_ref)):
-        for h in range(q):
-            copy = pltpu.make_async_copy(
-                w.at[layer, pl.ds(h * width, width), :], wbuf.at[m, h], wsem.at[m, h]
+    collects = z // half == c
+    columns = wobuf.shape[1]
+    pieces = 3
+    piece = columns // pieces
+
+    params = [
+        pltpu.make_async_copy(src.at[layer], dst, ssem.at[i])
+        for i, (src, dst) in enumerate(
+            (
+                (decay_ref, decay), (freq_ref, freq), (ire_ref, i_re), (iim_ref, i_im),
+                (rre_ref, r_re), (rim_ref, r_im), (sre_ref, h_re), (sim_ref, h_im),
             )
-            copy.start()
+        )
+    ]
+    for copy in params:
+        copy.start()
+    def fetch(n):
+        return pltpu.make_async_copy(
+            wout_ref.at[layer, :, pl.ds(pl.multiple_of(c * columns + n * piece, 128), piece)],
+            wobuf.at[:, pl.ds(n * piece, piece)],
+            osem.at[n],
+        )
 
     barrier = pltpu.get_barrier_semaphore()
     for e in range(dp):
@@ -259,7 +285,15 @@
     greet(barrier, {"tp": z * q + other})
     greet(barrier, {"dp": partner})
     greet(barrier, {"dp": far})
-    pl.semaphore_wait(barrier, dp + 3 - home.astype(jnp.int32))
+
+    @pl.when(collects)
+    def _():
+        for o in range(1, dp):
+            greet(barrier, {"tp": ((z + o) % dp) * q + y})
+
+    pl.semaphore_wait(
+        barrier, dp + 3 + half - home.astype(jnp.int32) - collects.astype(jnp.int32)
+    )
 
     upper = z // half
     order = [
@@ -287,11 +321,100 @@
 
     def across(src, e, slot):
         return remote(
-            src, xg.at[slot, e], ysend.at[e], yrecv.at[e], {"tp": z * q + other}
+            src, xg.at[slot, e], across_send.at[e], across_recv.at[e], {"tp": z * q + other}
         )
 
     slots = [d, partner, far, beside]
+    many, cut = 4, 4
+
+    def mixing(o, carry):
+        for i in range(0, gs, cut):
+            total = [None] * cut
+            for p in range(0, states, 8):
+                rows = slice(p, p + 8)
+                left_re, left_im = r_re[o, rows, :], r_im[o, rows, :]
+                for j in range(cut):
+                    term = left_re * b_re[i + j, rows, :] - left_im * b_im[i + j, rows, :]
+                    total[j] = term if p == 0 else total[j] + term
+            for j in range(cut):
+                mix[o, i + j : i + j + 1, :] = jnp.sum(total[j], axis=0, keepdims=True)
+        return carry
+
+    def recall(step, carry):
+        first = step * many
+        for p in range(0, states, 8):
+            rows = slice(p, p + 8)
+            pole_re, pole_im = a_re[rows, :], a_im[rows, :]
+            for b in range(many):
+                o_re, o_im = h_re[first + b, rows, :], h_im[first + b, rows, :]
+                h_re[first + b, rows, :] = pole_re * o_re - pole_im * o_im
+                h_im[first + b, rows, :] = pole_re * o_im + pole_im * o_re
+        for i in range(0, gs, cut):
+            total = [[None] * many for _ in range(cut)]
+            for p in range(0, states, 8):
+                rows = slice(p, p + 8)
+                n_re = [h_re[first + b, rows, :] for b in range(many)]
+                n_im = [h_im[first + b, rows, :] for b in range(many)]
+                for j in range(cut):
+                    left_re, left_im = r_re[i + j, rows, :], r_im[i + j, rows, :]
+                    for b in range(many):
+                        term = left_re * n_re[b] - left_im * n_im[b]
+                        total[j][b] = term if p == 0 else total[j][b] + term
+            for j in range(cut):
+                for b in range(many):
+                    y0[first + b, i + j : i + j + 1, :] = jnp.sum(
+                        total[j][b], axis=0, keepdims=True
+                    )
+        return carry
+
+    def push(step, carry):
+        first = step * many
+        for p in range(0, states, 8):
+            rows = slice(p, p + 8)
+            n_re = [h_re[first + b, rows, :] for b in range(many)]
+            n_im = [h_im[first + b, rows, :] for b in range(many)]
+            for i in range(gs):
+                in_re, in_im = b_re[i, rows, :], b_im[i, rows, :]
+                for b in range(many):
+                    u = ub[first + b, i : i + 1, :]
+                    n_re[b] = n_re[b] + in_re * u
+                    n_im[b] = n_im[b] + in_im * u
+            for b in range(many):
+                h_re[first + b, rows, :] = n_re[b]
+                h_im[first + b, rows, :] = n_im[b]
+        return carry
+
+    for copy in params[:4]:
+        copy.wait()
+    step = jnp.exp(logstep_ref[layer : layer + 1, :])
+    lam_re, lam_im = -decay[...], freq[...]
+    magnitude = jnp.exp(lam_re * step)
+    angle = lam_im * step
+    pole_re, pole_im = magnitude * jnp.cos(angle), magnitude * jnp.sin(angle)
+    denom = lam_re * lam_re + lam_im * lam_im
+    num_re = pole_re - 1.0
+    a_re[...] = pole_re
+    a_im[...] = pole_im
+    zoh_re = (num_re * lam_re + pole_im * lam_im) / denom
+    zoh_im = (pole_im * lam_re - num_re * lam_im) / denom
+    flat_re, flat_im = i_re.reshape(states * gs, groups), i_im.reshape(states * gs, groups)
+    for i in range(gs):
+        col = pl.ds(i, states, stride=gs)
+        in_re, in_im = flat_re[col, :], flat_im[col, :]
+        b_re[i] = zoh_re * in_re - zoh_im * in_im
+        b_im[i] = zoh_re * in_im + zoh_im * in_re
+    for copy in params[4:]:
+        copy.wait()
+    for m, w in enumerate((win_ref, wgate_ref)):
+        for h in range(q):
+            pltpu.make_async_copy(
+                w.at[layer, pl.ds(h * width, width), :], wbuf.at[m, h], wsem.at[m, h]
+            ).start()
+    lax.fori_loop(0, gs, mixing, 0)
+    steps = batch // many
+    marks = [(i * steps) // dp for i in range(dp + 1)]
     for i in range(dp):
+        lax.fori_loop(marks[i], marks[i + 1], recall, 0)
         e = slots[i]
         if i == 0:
             @pl.when(home)
@@ -307,14 +430,14 @@
             across(xg.at[y, e], e, y).start()
 
     def scale(h, first):
-        gain = gain_ref[h]
+        gain = gain_ref[layer, pl.ds(d * q + h, 1), :]
         for e in range(dp):
             xf = xg[h, e].astype(jnp.float32)
             total = jnp.broadcast_to(jnp.sum(xf * xf, axis=1, keepdims=True), squares.shape[1:])
             squares[e] = total if first else squares[e] + total
             scaled[e * batch : (e + 1) * batch, :] = (xf * gain).astype(jnp.bfloat16)
 
-    cut = 256
+    tile = channels // 2
 
     scale(y, True)
     for m in range(2):
@@ -323,20 +446,26 @@
         ).wait()
 
         def first(n, carry):
-            cols = pl.ds(pl.multiple_of(n * cut, cut), cut)
+            cols = pl.ds(pl.multiple_of(n * tile, 128), tile)
             part = jnp.dot(scaled[...], wbuf[m, y, :, cols], preferred_element_type=jnp.float32)
-            acc[m, :, :, cols] = part.reshape(dp, batch, cut)
+            acc[m, :, :, cols] = part.reshape(dp, batch, tile)
             return carry
 
-        lax.fori_loop(0, channels // cut, first, 0)
+        lax.fori_loop(0, channels // tile, first, 0)
+
+    for n in range(pieces):
+        fetch(n).start()
+    flat = y0.reshape(batch * gs, groups)
+    for i in range(gs):
+        y0p[i] = flat[pl.ds(i, batch, stride=gs), :]
 
     for i in range(dp):
-        e = slots[i]
-        across(x_ref, e, other).wait_recv()
+        across(x_ref, slots[i], other).wait_recv()
     scale(other, False)
     for h in range(half):
         sq_out1[h] = squares[2 * h + 1 - c]
-    remote(sq_out1, sq_in1, send1.at[2], recv1.at[2], {"dp": partner}).start()
+    sq1 = remote(sq_out1, sq_in1, send1.at[2], recv1.at[2], {"dp": partner})
+    sq1.start()
 
     def stage1(m):
         return remote(out1.at[m], in1.at[m], send1.at[m], recv1.at[m], {"dp": partner})
@@ -350,19 +479,19 @@
         ).wait()
 
         def second(n, carry):
-            cols = pl.ds(pl.multiple_of(n * cut, cut), cut)
+            cols = pl.ds(pl.multiple_of(n * tile, 128), tile)
             part = jnp.dot(
                 scaled[...], wbuf[m, other, :, cols], preferred_element_type=jnp.float32
             )
-            acc[m, :, :, cols] = acc[m, :, :, cols] + part.reshape(dp, batch, cut)
+            acc[m, :, :, cols] = acc[m, :, :, cols] + part.reshape(dp, batch, tile)
             for h in range(half):
                 out1[m, h, :, cols] = acc[m, 2 * h + 1 - c, :, cols].astype(jnp.bfloat16)
             return carry
 
-        lax.fori_loop(0, channels // cut, second, 0)
+        lax.fori_loop(0, channels // tile, second, 0)
         stage1(m).start()
 
-    remote(sq_out1, sq_in1, send1.at[2], recv1.at[2], {"dp": partner}).wait()
+    sq1.wait()
     sq_out2[...] = squares[far] + sq_in1[1 - x]
     sq2 = remote(sq_out2, sq_in2, send2.at[2], recv2.at[2], {"dp": far})
     sq2.start()
@@ -374,10 +503,137 @@
     sq2.wait()
     meansq = (squares[d] + sq_in1[x] + sq_in2[...])[:, :1] / features
     inverse = lax.rsqrt(meansq + 1e-06)
-    for m, result in enumerate((drive_ref, gate_ref)):
-        stage2(m).wait()
-        result[...] = (acc[m, d] + in2[m].astype(jnp.float32)) * inverse
-
+    stage2(0).wait()
+    drive = (acc[0, d] + in2[0].astype(jnp.float32)) * inverse
+    unat[...] = drive
+    flip[...] = drive.T
+    for i in range(gs):
+        u3[i] = flip[pl.ds(i, groups, stride=gs), :].T
+
+    def respond(n, carry):
+        rows = pl.ds(pl.multiple_of(n * 8, 8), 8)
+        u = [u3[i, rows, :] for i in range(gs)]
+        for o in range(gs):
+            total = y0p[o, rows, :]
+            for i in range(gs):
+                total = total + mix[o, i : i + 1, :] * u[i]
+            y3[o, rows, :] = total
+        return carry
+
+    lax.fori_loop(0, batch // 8, respond, 0)
+    for i in range(gs):
+        flipy[pl.ds(i, groups, stride=gs), :] = y3[i].T
+    read = flipy[...].T + skip_ref[layer : layer + 1, :] * unat[...]
+    stage2(1).wait()
+    gate = (acc[1, d] + in2[1].astype(jnp.float32)) * inverse
+    gated[...] = (jax.nn.gelu(read) * jax.nn.sigmoid(gate)).astype(jnp.bfloat16)
+
+    swap = remote(gated, both.at[c], swap_send, swap_recv, {"dp": partner})
+    swap.start()
+    both[c] = gated[...]
+    flat_u = u3.reshape(gs * batch, groups)
+    for b in range(batch):
+        ub[b] = flat_u[pl.ds(b, gs, stride=batch), :]
+    remote(gated, both.at[1 - c], swap_send, swap_recv, {"dp": partner}).wait_recv()
+    first_turn = jnp.where(c == 0, jnp.where(z == 0, 1, 0), jnp.where(z == dp - 1, 0, 1))
+    turns = [first_turn, 1 - first_turn]
+
+    def over_y(k, e):
+        return remote(
+            ybuf.at[k, e], yin.at[k, e], ysend.at[k, e], yrecv.at[k, e], {"tp": z * q + other}
+        )
+
+    def over_z(k, e):
+        return remote(
+            zbuf.at[k, e],
+            zin.at[z, e],
+            zsend.at[k, e],
+            zrecv.at[z, e],
+            {"tp": (half * c + k) * q + y},
+        )
+
+    rows = both[...].reshape(2 * batch, channels)
+
+    def multiply(n):
+        pltpu.make_async_copy(
+            wout_ref.at[layer, :, pl.ds(0, piece)], wobuf.at[:, pl.ds(0, piece)], osem.at[n]
+        ).wait()
+        span = pl.ds(pl.multiple_of(n * piece, 128), piece)
+        prod[:, span] = jnp.dot(rows, wobuf[:, span], preferred_element_type=jnp.float32)
+
+    def send_over_y(k):
+        for static in range(half):
+            @pl.when(k == static)
+            def _():
+                for j in range(static * q, (static + 1) * q):
+                    for e in range(2):
+                        blocks[j, e] = prod[
+                            e * batch : (e + 1) * batch, j * width : (j + 1) * width
+                        ]
+        for e in range(2):
+            ybuf[k, e] = blocks[q * k + other, e].astype(jnp.bfloat16)
+            over_y(k, e).start()
+
+    multiply((pieces - 1) * first_turn)
+    multiply(1)
+    send_over_y(turns[0])
+    multiply((pieces - 1) * turns[1])
+    send_over_y(turns[1])
+    lax.fori_loop(0, steps, push, 0)
+    results = [
+        pltpu.make_async_copy(h_re, nre_ref.at[layer], psem.at[0]),
+        pltpu.make_async_copy(h_im, nim_ref.at[layer], psem.at[1]),
+    ]
+    for copy in results:
+        copy.start()
+    for k in turns:
+        mine = half * c + k == z
+        for e in range(2):
+            over_y(k, e).wait_recv()
+            total = blocks[q * k + y, e] + yin[k, e].astype(jnp.float32)
+
+            @pl.when(mine)
+            def _():
+                own[e] = total
+
+            @pl.when(jnp.logical_not(mine))
+            def _():
+                zbuf[k, e] = total.astype(jnp.bfloat16)
+                over_z(k, e).start()
+
+    def finish(total):
+        if layer == LAYERS - 1:
+            out_ref[...] = total
+        else:
+            out_ref[...] = (x_ref[...].astype(jnp.float32) + total).astype(jnp.bfloat16)
+
+    final = remote(last, last_in, fsend, frecv, {"dp": partner})
+
+    def gathered(e):
+        total = own[e]
+        for o in range(1, dp):
+            source = (z + o) % dp
+            remote(
+                zbuf.at[0, 0], zin.at[source, e], zsend.at[0, 0], zrecv.at[source, e],
+                {"dp": partner},
+            ).wait_recv()
+            total = total + zin[source, e].astype(jnp.float32)
+        return total
+
+    @pl.when(collects)
+    def _():
+        last[...] = gathered(1 - c)
+        final.start()
+        finish(gathered(c))
+        final.wait_send()
+
+    @pl.when(jnp.logical_not(collects))
+    def _():
+        final.wait_recv()
+        finish(last_in[...])
+
+    for copy in results:
+        copy.wait()
     for i in range(dp - 1):
         spread(i).wait_send()
 
@@ -387,21 +643,40 @@
 
     for i in range(dp):
         across(x_ref, slots[i], y).wait_send()
-
-
-def project(layer, x, gain, w_input, w_gating, tp, dp, features, ident):
+    swap.wait_send()
+    for k in range(2):
+        for e in range(2):
+            over_y(k, e).wait_send()
+
+            @pl.when(half * c + k != z)
+            def _():
+                over_z(k, e).wait_send()
+
+
+def layer_step(
+    layer, x, gain, skip, w_input, w_gating, w_output, log_step, eigen, state, earlier, tp, dp, ident
+):
     batch, width = x.shape
     channels = w_input.shape[2]
+    states, groups = eigen[0].shape[1:]
+    gs = channels // groups
+    features = w_output.shape[2]
     q = tp // dp
     half = dp // 2
     bf, f32 = jnp.bfloat16, jnp.float32
     vmem = pl.BlockSpec(memory_space=pltpu.VMEM)
     dma = pltpu.SemaphoreType.DMA
+    operands = [
+        x, gain, skip, w_input, w_gating, w_output, log_step, *eigen, *state, *earlier
+    ]
+    aliases = {len(operands) - 2: 1, len(operands) - 1: 2} if earlier else {}
     return pl.pallas_call(
-        functools.partial(project_kernel, layer, tp, dp, features),
-        out_shape=[jax.ShapeDtypeStruct((batch, channels), f32)] * 2,
-        in_specs=[vmem, vmem, ANY, ANY],
-        out_specs=[vmem, vmem],
+        functools.partial(layer_kernel, layer, tp, dp, features, len(earlier)),
+        out_shape=[jax.ShapeDtypeStruct((batch, width), f32 if layer == LAYERS - 1 else bf)]
+        + [jax.ShapeDtypeStruct(a.shape, f32) for a in state],
+        in_specs=[vmem] * 3 + [ANY] * 3 + [vmem] + [ANY] * (len(operands) - 7),
+        out_specs=[vmem, ANY, ANY],
+        input_output_aliases=aliases,
         scratch_shapes=[
             pltpu.VMEM((q, dp, batch, width), bf),
             pltpu.VMEM((2, q, width, channels), bf),
@@ -416,161 +691,28 @@
             pltpu.VMEM((half, batch, 128), f32),
             pltpu.VMEM((batch, 128), f32),
             pltpu.VMEM((batch, 128), f32),
-            dma((2, q)),
-            dma((dp,)),
-            dma((dp,)),
-            dma((dp,)),
-            dma((dp,)),
-            dma((3,)),
-            dma((3,)),
-            dma((3,)),
-            dma((3,)),
-        ],
-        compiler_params=pltpu.CompilerParams(
-            collective_id=ident, has_side_effects=True, vmem_limit_bytes=62 * 2**20
-        ),
-        name=f"project_{layer}",
-    )(x, gain, w_input, w_gating)
-
-
-def merge_kernel(
-    layer, tp, dp,
-    z_ref, x_ref, w_ref, out_ref,
-    both, wbuf, prod, blocks, ybuf, yin, zbuf, zin, own, last, last_in,
-    wsem, psend, precv, ysend, yrecv, zsend, zrecv, fsend, frecv,
-):
-    q = tp // dp
-    half = dp // 2
-    t, d = lax.axis_index("tp"), lax.axis_index("dp")
-    z, y = t // q, t % q
-    x, c = d // 2, d % 2
-    partner = 2 * x + 1 - c
-    other = 1 - y
-    batch, width = x_ref.shape
-    columns = wbuf.shape[1]
-    pieces = 3
-    piece = columns // pieces
-    collects = z // half == c
-
-    def fetch(n):
-        return pltpu.make_async_copy(
-            w_ref.at[layer, :, pl.ds(pl.multiple_of(c * columns + n * piece, 128), piece)],
-            wbuf.at[:, pl.ds(n * piece, piece)],
-            wsem.at[n],
-        )
-
-    for n in range(pieces):
-        fetch(n).start()
-
-    barrier = pltpu.get_barrier_semaphore()
-    greet(barrier, {"dp": partner})
-    greet(barrier, {"tp": z * q + other})
-
-    @pl.when(collects)
-    def _():
-        for o in range(1, dp):
-            greet(barrier, {"tp": ((z + o) % dp) * q + y})
-
-    pl.semaphore_wait(barrier, 2 + half - collects.astype(jnp.int32))
-
-    swap = remote(z_ref, both.at[c], psend, precv, {"dp": partner})
-    swap.start()
-    both[c] = z_ref[...]
-    remote(z_ref, both.at[1 - c], psend, precv, {"dp": partner}).wait_recv()
-    rows = both[...].reshape(2 * batch, both.shape[2])
-    for n in range(pieces):
-        fetch(n).wait()
-        span = slice(n * piece, (n + 1) * piece)
-        prod[:, span] = jnp.dot(rows, wbuf[:, span], preferred_element_type=jnp.float32)
-    for j in range(half * q):
-        for e in range(2):
-            blocks[j, e] = prod[e * batch : (e + 1) * batch, j * width : (j + 1) * width]
-
-    first = jnp.where(c == 0, jnp.where(z == 0, 1, 0), jnp.where(z == dp - 1, 0, 1))
-    turns = [first, 1 - first]
-
-    def over_y(k, e):
-        return remote(
-            ybuf.at[k, e], yin.at[k, e], ysend.at[k, e], yrecv.at[k, e], {"tp": z * q + other}
-        )
-
-    def over_z(k, e):
-        return remote(
-            zbuf.at[k, e],
-            zin.at[z, e],
-            zsend.at[k, e],
-            zrecv.at[z, e],
-            {"tp": (half * c + k) * q + y},
-        )
-
-    for k in turns:
-        for e in range(2):
-            ybuf[k, e] = blocks[q * k + other, e].astype(jnp.bfloat16)
-            over_y(k, e).start()
-    for k in turns:
-        mine = half * c + k == z
-        for e in range(2):
-            over_y(k, e).wait_recv()
-            total = blocks[q * k + y, e] + yin[k, e].astype(jnp.float32)
-
-            @pl.when(mine)
-            def _():
-                own[e] = total
-
-            @pl.when(jnp.logical_not(mine))
-            def _():
-                zbuf[k, e] = total.astype(jnp.bfloat16)
-                over_z(k, e).start()
-
-    final = remote(last, last_in, fsend, frecv, {"dp": partner})
-
-    def gathered(e):
-        total = own[e]
-        for o in range(1, dp):
-            source = (z + o) % dp
-            remote(
-                zbuf.at[0, 0], zin.at[source, e], zsend.at[0, 0], zrecv.at[source, e],
-                {"dp": partner},
-            ).wait_recv()
-            total = total + zin[source, e].astype(jnp.float32)
-        return total
-
-    @pl.when(collects)
-    def _():
-        last[...] = gathered(1 - c)
-        final.start()
-        out_ref[...] = (x_ref[...].astype(jnp.float32) + gathered(c)).astype(jnp.bfloat16)
-        final.wait_send()
-
-    @pl.when(jnp.logical_not(collects))
-    def _():
-        final.wait_recv()
-        out_ref[...] = (x_ref[...].astype(jnp.float32) + last_in[...]).astype(jnp.bfloat16)
-
-    swap.wait_send()
-    for k in range(2):
-        for e in range(2):
-            over_y(k, e).wait_send()
-
-            @pl.when(half * c + k != z)
-            def _():
-                over_z(k, e).wait_send()
-
-
-def merge(layer, gated, x, w_output, tp, dp, ident):
-    batch, width = x.shape
-    channels, features = w_output.shape[1:]
-    q = tp // dp
-    half = dp // 2
-    bf, f32 = jnp.bfloat16, jnp.float32
-    vmem = pl.BlockSpec(memory_space=pltpu.VMEM)
-    dma = pltpu.SemaphoreType.DMA
-    return pl.pallas_call(
-        functools.partial(merge_kernel, layer, tp, dp),
-        out_shape=jax.ShapeDtypeStruct((batch, width), bf),
-        in_specs=[vmem, vmem, ANY],
-        out_specs=vmem,
-        scratch_shapes=[
+            pltpu.VMEM((states, groups), f32),
+            pltpu.VMEM((states, groups), f32),
+            pltpu.VMEM((states, gs, groups), f32),
+            pltpu.VMEM((states, gs, groups), f32),
+            pltpu.VMEM((states, groups), f32),
+            pltpu.VMEM((states, groups), f32),
+            pltpu.VMEM((gs, states, groups), f32),
+            pltpu.VMEM((gs, states, groups), f32),
+            pltpu.VMEM((gs, states, groups), f32),
+            pltpu.VMEM((gs, states, groups), f32),
+            pltpu.VMEM((batch, states, groups), f32),
+            pltpu.VMEM((batch, states, groups), f32),
+            pltpu.VMEM((gs, gs, groups), f32),
+            pltpu.VMEM((batch, gs, groups), f32),
+            pltpu.VMEM((gs, batch, groups), f32),
+            pltpu.VMEM((gs, batch, groups), f32),
+            pltpu.VMEM((gs, batch, groups), f32),
+            pltpu.VMEM((batch, gs, groups), f32),
+            pltpu.VMEM((channels, batch), f32),
+            pltpu.VMEM((channels, batch), f32),
+            pltpu.VMEM((batch, channels), f32),
+            pltpu.VMEM((batch, channels), bf),
             pltpu.VMEM((2, batch, channels), bf),
             pltpu.VMEM((channels, features // 2), bf),
             pltpu.VMEM((2 * batch, features // 2), f32),
@@ -582,7 +724,18 @@
             pltpu.VMEM((2, batch, width), f32),
             pltpu.VMEM((batch, width), f32),
             pltpu.VMEM((batch, width), f32),
+            dma((2, q)),
+            dma((dp,)),
+            dma((dp,)),
+            dma((dp,)),
+            dma((dp,)),
             dma((3,)),
+            dma((3,)),
+            dma((3,)),
+            dma((3,)),
+            dma((8,)),
+            dma((3,)),
+            dma((2,)),
             dma,
             dma,
             dma((half, 2)),
@@ -595,8 +748,8 @@
         compiler_params=pltpu.CompilerParams(
             collective_id=ident, has_side_effects=True, vmem_limit_bytes=62 * 2**20
         ),
-        name=f"merge_{layer}",
-    )(gated, x, w_output)
+        name=f"layer_{layer}",
+    )(*operands)
 
 
 def on_device(
@@ -626,6 +779,27 @@
     q = tp // dp
     d = lax.axis_index("dp")
 
+    if q == 2 and dp == 4:
+        eigen = (
+            jnp.swapaxes(decay_rate, 1, 2),
+            jnp.swapaxes(frequency, 1, 2),
+            jnp.transpose(in_real, (0, 2, 3, 1)),
+            jnp.transpose(in_imag, (0, 2, 3, 1)),
+            jnp.transpose(readout_real_matrix, (0, 2, 3, 1)),
+            jnp.transpose(readout_imag_matrix, (0, 2, 3, 1)),
+        )
+        state = (jnp.swapaxes(state_real, 2, 3), jnp.swapaxes(state_imag, 2, 3))
+        gain = gains.reshape(LAYERS, tp, width)
+        shard, news = tokens, ()
+        for layer in range(LAYERS):
+            before = shard
+            shard, *news = layer_step(
+                layer, shard, gain, skip_gain, w_input, w_gating, w_output,
+                log_step, eigen, state, tuple(news), tp, dp, layer + 1,
+            )
+        shard = (before.astype(jnp.float32) + shard).astype(jnp.bfloat16)
+        return shard, jnp.swapaxes(news[0], 2, 3), jnp.swapaxes(news[1], 2, 3)
+
     step = jnp.exp(log_step)[:, None, :]
     lam_re = -jnp.swapaxes(decay_rate, 1, 2)
     lam_im = jnp.swapaxes(frequency, 1, 2)
@@ -649,21 +823,7 @@
 
     shard = tokens
     news = ()
-    paired = q == 2 and dp == 4
     for layer in range(LAYERS):
-        if paired:
-            drive, gate = project(
-                layer, shard, my_gains[layer], w_input, w_gating, tp, dp, features, 2 * layer + 1
-            )
-            u = jnp.swapaxes(drive.reshape(batch, groups, GS), 1, 2)
-            n_re, n_im, y = state_step(
-                layer, u, abar_re, abar_im, bbar_re, bbar_im, r_re, r_im, s_re, s_im, news
-            )
-            news = (n_re, n_im)
-            y = jnp.swapaxes(y, 1, 2).reshape(batch, channels) + skip_gain[layer][None] * drive
-            z = (jax.nn.gelu(y) * jax.nn.sigmoid(gate)).astype(jnp.bfloat16)
-            shard = merge(layer, z, shard, w_output, tp, dp, 2 * layer + 2)
-            continue
         got = gather(shard, tp, dp, 3 * layer + 1).reshape(q, dp * batch, width)
         xf = got.astype(jnp.float32)
         squares = jnp.sum(xf * xf, axis=(0, 2))

time: 163 us -> 123 us (0.75)
  Pallas kernels: 142 us -> 113 us
  local copies, waits for them, and re-layouts: 13.4 us -> 7.42 us
  other arithmetic: 6.68 us -> 1.6 us
    pallas_call x6 -> x2, Pallas kernels: 142 us -> 113 us  [layer_step(): pl.pallas_call(functools.partial(layer_kernel, layer, tp, dp, features, l...]
    unnamed x11 -> x6, local copies, waits for them, and re-layouts: 1.57 us -> 5.79 us
    add x1 -> x0, other arithmetic: 3.2 us -> none  [on_device(): bbar_im = zoh_re * i_im + zoh_im * i_re]
    transpose x2 -> x0, local copies, waits for them, and re-layouts: 2.83 us -> none  [on_device(): jnp.swapaxes(y, 1, 2).reshape(batch, channels)]
    pallas_call x2 -> x0, local copies, waits for them, and re-layouts: 2.45 us -> none  [project(): pl.pallas_call(functools.partial(project_kernel, layer, tp, dp, features)...]
    div x1 -> x0, other arithmetic: 1.81 us -> none  [on_device(): zoh_re = ((num_re * lam_re + abar_im * lam_im) / denom)[:, None]]
    slice x2 -> x0, local copies, waits for them, and re-layouts: 1.74 us -> none  [the longest x1 0.92 us: on_device(): my_gains[layer]]
where the time goes in v2:
time: 123 us; the launch traced here: 122 us
  Pallas kernels  113 us (92%)
  local copies, waits for them, and re-layouts  7.42 us (6%)
  other arithmetic  1.6 us (1%)
    pallas_call x2, Pallas kernels, layer_step(): pl.pallas_call(functools.partial(layer_kernel, layer, tp, dp, features, l...  113 us
    unnamed x6, local copies, waits for them, and re-layouts  5.79 us

profile of v2, /device:TPU:15, one launch (start us, length us, event | category | flops | bytes accessed | tf_op | source)
XLA Modules:
  0.0 122.4 jit_solution(12215400228653343433)
XLA Ops:
  0.6 1.6 %reshape.9.gain_ref = f32[2,8,1056]{2,1,0:T(8,128)} reshape(f32[2,8448]{1,0:T(2,128)} %param.16) | data formatting | bytes 135168 | tf_op jit(solution)/shard_map/reshape | solution.py:792
  2.3 57.6 %layer_0.1 = (bf16[48,1056]{1,0:T(8,128)(2,1)}, f32[2,48,64,96]{3,2,1,0:T(8,128)}, f32[2,48,64,96]{3,2,1,0:T(8,128)}) custom-call(bf16[48,1056]{1,0:T(8,128)(2,1)} %x_ref.1, f32[2,8,1056]{2,1,0:T(8,128)} %reshape.9.gain_ref, f32[2,1536]{1,0:T(2,128)} %skip_ref.3, bf16[2,2112,1536]{2,1,0:T(8,128)(2,1)} %win_ref.3, bf16[2,2112,1536]{2,1,0:T(8,128)(2,1)} %wgate_ref.3, ...), custom_call_target="tpu_custom_call" | custom-call | tf_op jit(solution)/shard_map/layer_0/pallas_call | solution.py:673
  59.9 0.0 copy-start.1
  59.9 55.1 %layer_1.1 = (f32[48,1056]{1,0:T(8,128)}, f32[2,48,64,96]{3,2,1,0:T(8,128)}, f32[2,48,64,96]{3,2,1,0:T(8,128)}) custom-call(bf16[48,1056]{1,0:T(8,128)(2,1)} %get-tuple-element.9.x_ref, f32[2,8,1056]{2,1,0:T(8,128)} %reshape.9.gain_ref, f32[2,1536]{1,0:T(2,128)} %skip_ref.3, ...), custom_call_target="tpu_custom_call", output_to_operand_aliasing={{1}: (15, {}), {2}: (16, {})} | custom-call | tf_op jit(solution)/shard_map/layer_1/pallas_call | solution.py:673
  115.0 0.0 copy-done.1
  115.0 1.6 %add_convert_fusion = bf16[48,1056]{1,0:T(8,128)(2,1)} fusion(f32[48,1056]{1,0:T(8,128)} %get-tuple-element.12, bf16[48,1056]{1,0:T(8,128)(2,1)S(1)} %copy-done.1), kind=kLoop, calls=%fused_computation | loop fusion | flops 152064 | bytes 405504 | tf_op jit(solution)/shard_map/convert_element_type | solution.py:800
  116.6 0.0 copy-start
  116.6 4.1 %copy.24 = f32[2,48,96,64]{2,3,1,0:T(8,128)} copy(f32[2,48,96,64]{2,3,1,0:T(8,128)} %bitcast.14) | data formatting | bytes 4718592
  120.7 0.0 copy-done
  120.7 1.7 %copy.25 = f32[2,48,96,64]{2,3,1,0:T(8,128)} copy(f32[2,48,96,64]{2,3,1,0:T(8,128)S(1)} %bitcast.15) | data formatting | bytes 4718592
Async XLA Ops:
  59.9 55.1 %copy-start.1 = (bf16[48,1056]{1,0:T(8,128)(2,1)S(1)}, bf16[48,1056]{1,0:T(8,128)(2,1)}, u32[]{:S(2)}) copy-start(bf16[48,1056]{1,0:T(8,128)(2,1)} %get-tuple-element.9.x_ref) | copy-start | bytes 304132
  116.6 4.1 %copy-start = (f32[2,48,64,96]{3,2,1,0:T(8,128)S(1)}, f32[2,48,64,96]{3,2,1,0:T(8,128)}, u32[]{:S(2)}) copy-start(f32[2,48,64,96]{3,2,1,0:T(8,128)} %get-tuple-element.14) | copy-start | bytes 7077892

commit v3 on v2

--- a/solution.py
+++ b/solution.py
@@ -233,7 +233,7 @@
     (
         xg, wbuf, scaled, acc, squares,
         out1, in1, out2, in2, sq_out1, sq_in1, sq_out2, sq_in2,
-        decay, freq, i_re, i_im,
+        gain_rows, decay, freq, i_re, i_im,
         a_re, a_im, b_re, b_im, r_re, r_im, h_re, h_im,
         mix, y0, y0p, y3, u3, ub, flip, flipy, unat, gated,
         both, wobuf, prod, blocks, ybuf, yin, zbuf, zin, own, last, last_in,
@@ -384,6 +384,8 @@
                 h_im[first + b, rows, :] = n_im[b]
         return carry
 
+    for j in range(tp):
+        gain_rows[j] = gain_ref[layer : layer + 1, j * width : (j + 1) * width]
     for copy in params[:4]:
         copy.wait()
     step = jnp.exp(logstep_ref[layer : layer + 1, :])
@@ -430,14 +432,14 @@
             across(xg.at[y, e], e, y).start()
 
     def scale(h, first):
-        gain = gain_ref[layer, pl.ds(d * q + h, 1), :]
+        gain = gain_rows[d * q + h]
         for e in range(dp):
             xf = xg[h, e].astype(jnp.float32)
             total = jnp.broadcast_to(jnp.sum(xf * xf, axis=1, keepdims=True), squares.shape[1:])
             squares[e] = total if first else squares[e] + total
             scaled[e * batch : (e + 1) * batch, :] = (xf * gain).astype(jnp.bfloat16)
 
-    tile = channels // 2
+    tile = channels
 
     scale(y, True)
     for m in range(2):
@@ -579,16 +581,19 @@
     send_over_y(turns[0])
     multiply((pieces - 1) * turns[1])
     send_over_y(turns[1])
-    lax.fori_loop(0, steps, push, 0)
     results = [
         pltpu.make_async_copy(h_re, nre_ref.at[layer], psem.at[0]),
         pltpu.make_async_copy(h_im, nim_ref.at[layer], psem.at[1]),
     ]
-    for copy in results:
-        copy.start()
-    for k in turns:
+    early = 2 * steps // 3
+    for i, k in enumerate(turns):
         mine = half * c + k == z
         for e in range(2):
+            if i == 0:
+                lax.fori_loop(e * early, steps if e else early, push, 0)
+                if e:
+                    for copy in results:
+                        copy.start()
             over_y(k, e).wait_recv()
             total = blocks[q * k + y, e] + yin[k, e].astype(jnp.float32)
 
@@ -691,6 +696,7 @@
             pltpu.VMEM((half, batch, 128), f32),
             pltpu.VMEM((batch, 128), f32),
             pltpu.VMEM((batch, 128), f32),
+            pltpu.VMEM((tp, 1, width), f32),
             pltpu.VMEM((states, groups), f32),
             pltpu.VMEM((states, groups), f32),
             pltpu.VMEM((states, gs, groups), f32),
@@ -752,6 +758,66 @@
     )(*operands)
 
 
+def finish_kernel(
+    sum_ref, x_ref, re_ref, im_ref, out_ref, nre_ref, nim_ref,
+    total, x, mixed, held, rsem, wsem, small,
+):
+    layers, batch = re_ref.shape[:2]
+    pieces = rsem.shape[2]
+    size = batch // pieces
+    moves = []
+    for n in range(pieces):
+        for layer in range(layers):
+            for i, (src, dst) in enumerate(((re_ref, nre_ref), (im_ref, nim_ref))):
+                part = (layer, pl.ds(n * size, size))
+                take = pltpu.make_async_copy(
+                    src.at[part], held.at[i].at[part], rsem.at[i, layer, n]
+                )
+                take.start()
+                put = pltpu.make_async_copy(
+                    held.at[i].at[part], dst.at[part], wsem.at[i, layer, n]
+                )
+                moves.append((take, put))
+    loads = [
+        pltpu.make_async_copy(sum_ref, total, small.at[0]),
+        pltpu.make_async_copy(x_ref, x, small.at[1]),
+    ]
+    for copy in loads:
+        copy.start()
+    for take, put in moves:
+        take.wait()
+        put.start()
+    for copy in loads:
+        copy.wait()
+    mixed[...] = (x[...].astype(jnp.float32) + total[...]).astype(jnp.bfloat16)
+    result = pltpu.make_async_copy(mixed, out_ref, small.at[2])
+    result.start()
+    for take, put in moves:
+        put.wait()
+    result.wait()
+
+
+def finish(total, x, n_re, n_im):
+    pieces = 4
+    return pl.pallas_call(
+        finish_kernel,
+        out_shape=[jax.ShapeDtypeStruct(a.shape, a.dtype) for a in (x, n_re, n_im)],
+        in_specs=[ANY] * 4,
+        out_specs=[ANY] * 3,
+        scratch_shapes=[
+            pltpu.VMEM(total.shape, total.dtype),
+            pltpu.VMEM(x.shape, x.dtype),
+            pltpu.VMEM(x.shape, x.dtype),
+            pltpu.VMEM((2,) + n_re.shape, n_re.dtype),
+            pltpu.SemaphoreType.DMA((2, n_re.shape[0], pieces)),
+            pltpu.SemaphoreType.DMA((2, n_re.shape[0], pieces)),
+            pltpu.SemaphoreType.DMA((3,)),
+        ],
+        compiler_params=pltpu.CompilerParams(vmem_limit_bytes=62 * 2**20),
+        name="finish",
+    )(total, x, n_re, n_im)
+
+
 def on_device(
     tp,
     dp,
@@ -789,15 +855,14 @@
             jnp.transpose(readout_imag_matrix, (0, 2, 3, 1)),
         )
         state = (jnp.swapaxes(state_real, 2, 3), jnp.swapaxes(state_imag, 2, 3))
-        gain = gains.reshape(LAYERS, tp, width)
         shard, news = tokens, ()
         for layer in range(LAYERS):
             before = shard
             shard, *news = layer_step(
-                layer, shard, gain, skip_gain, w_input, w_gating, w_output,
+                layer, shard, gains, skip_gain, w_input, w_gating, w_output,
                 log_step, eigen, state, tuple(news), tp, dp, layer + 1,
             )
-        shard = (before.astype(jnp.float32) + shard).astype(jnp.bfloat16)
+        shard, *news = finish(shard, before, *news)
         return shard, jnp.swapaxes(news[0], 2, 3), jnp.swapaxes(news[1], 2, 3)
 
     step = jnp.exp(log_step)[:, None, :]

time: 123 us -> 116 us (0.943)
  local copies, waits for them, and re-layouts: 7.42 us -> 0 us
  other arithmetic: 1.6 us -> 0 us
    unnamed x6 -> x0, local copies, waits for them, and re-layouts: 5.79 us -> none
    pallas_call x0 -> x1, Pallas kernels: none -> 5.59 us  [finish(): pl.pallas_call(finish_kernel, out_shape=[jax.ShapeDtypeStruct(a.shape, a....]
    pallas_call x2, Pallas kernels: 113 us -> 109 us  [layer_step(): pl.pallas_call(functools.partial(layer_kernel, layer, tp, dp, features, l...]
    reshape x1 -> x0, local copies, waits for them, and re-layouts: 1.63 us -> none  [on_device(): gain = gains.reshape(LAYERS, tp, width)]
    convert_element_type x1 -> x0, other arithmetic: 1.6 us -> none  [on_device(): shard = (before.astype(jnp.float32) + shard).astype(jnp.bfloat16)]
where the time goes in v3:
time: 116 us; the launch traced here: 115 us
  Pallas kernels  114 us (98%)
    pallas_call x2, Pallas kernels, layer_step(): pl.pallas_call(functools.partial(layer_kernel, layer, tp, dp, features, l...  109 us
    pallas_call x1, Pallas kernels, finish(): pl.pallas_call(finish_kernel, out_shape=[jax.ShapeDtypeStruct(a.shape, a....  5.59 us

profile of v3, /device:TPU:15, one launch (start us, length us, event | category | flops | bytes accessed | tf_op | source)
XLA Modules:
  0.0 115.2 jit_solution(17765576802414279628)
XLA Ops:
  0.6 55.9 %layer_0.1 = (bf16[48,1056]{1,0:T(8,128)(2,1)}, f32[2,48,64,96]{3,2,1,0:T(8,128)}, f32[2,48,64,96]{3,2,1,0:T(8,128)}) custom-call(bf16[48,1056]{1,0:T(8,128)(2,1)} %x_ref.1, f32[2,8448]{1,0:T(2,128)} %gain_ref.3, f32[2,1536]{1,0:T(2,128)} %skip_ref.3, bf16[2,2112,1536]{2,1,0:T(8,128)(2,1)} %win_ref.3, bf16[2,2112,1536]{2,1,0:T(8,128)(2,1)} %wgate_ref.3, ...), custom_call_target="tpu_custom_call" | custom-call | tf_op jit(solution)/shard_map/layer_0/pallas_call | solution.py:678
  56.5 52.9 %layer_1.1 = (f32[48,1056]{1,0:T(8,128)}, f32[2,48,64,96]{3,2,1,0:T(8,128)}, f32[2,48,64,96]{3,2,1,0:T(8,128)}) custom-call(bf16[48,1056]{1,0:T(8,128)(2,1)} %get-tuple-element.12.x_ref, f32[2,8448]{1,0:T(2,128)} %gain_ref.3, f32[2,1536]{1,0:T(2,128)} %skip_ref.3, bf16[2,2112,1536]{2,1,0:T(8,128)(2,1)} %win_ref.3, ...), custom_call_target="tpu_custom_call", output_to_operand_aliasing={{1}: (15, {}), {2}: (16, {})} | custom-call | tf_op jit(solution)/shard_map/layer_1/pallas_call | solution.py:678
  109.4 5.6 %finish.1 = (bf16[48,1056]{1,0:T(8,128)(2,1)}, f32[2,48,64,96]{3,2,1,0:T(8,128)}, f32[2,48,64,96]{3,2,1,0:T(8,128)}) custom-call(f32[48,1056]{1,0:T(8,128)} %get-tuple-element.15.sum_ref, bf16[48,1056]{1,0:T(8,128)(2,1)} %get-tuple-element.12.x_ref, f32[2,48,64,96]{3,2,1,0:T(8,128)} %get-tuple-element.16.re_ref, f32[2,48,64,96]{3,2,1,0:T(8,128)} %get-tuple-element.17.im_ref), custom_call_target="tpu_custom_call" | custom-call | tf_op jit(solution)/shard_map/finish/pallas_call | solution.py:802
